TPU v7x, 512 devices: a whole 4x4x16 slice. The times are simulated.
512 devices in a mesh: fs: 64 (over z, y), tp: 8 (over x, core).
Axes of the slice: x: 4, y: 4, z: 16, core: 2. Of those that a mesh axis runs over, the one named last changes fastest.
Arguments:
- tokens: bfloat16 [20480, 2048], P('fs'), may hold values from -6 to 6
- w_gate: bfloat16 [2048, 5632], P('fs', 'tp'), may hold values from -0.125 to 0.125
- w_up: bfloat16 [2048, 5632], P('fs', 'tp'), may hold values from -0.125 to 0.125
- w_down: bfloat16 [5632, 2048], P('tp', 'fs'), may hold values from -0.078125 to 0.078125
- w_mix_in: bfloat16 [2048, 1024], P('fs', 'tp'), may hold values from -0.125 to 0.125
- w_mix_out: bfloat16 [1024, 2048], P('tp', 'fs'), may hold values from -0.1875 to 0.1875
- pool_w: bfloat16 [8, 128, 128], P('tp'), may hold values from -0.5 to 0.5
- pool_scale: bfloat16 [1024], P('tp'), may hold values from 0.099609375 to 1.8984375
- norm_gains: float32 [6, 2048], replicated, may hold values from 0.1 to 1.9
Outputs:
- layer_out: bfloat16 [20480, 2048], P(('fs', 'tp'))
All inputs are finite; a program needn't handle non-finite values.
Results may differ from a plain program's by a relative error of at most 0.018.
Values may be sent and summed in bfloat16 or wider, within the bound.
No kernel may reach another device: no remote copies, remote signals or barrier semaphores. Data moves between devices by JAX's collectives and lax.ppermute only.
A program may use at most 64 MiB of HBM per device.

v0:
```python
import functools

import jax
import jax.numpy as jnp
from jax import lax
from jax.experimental import pallas as pl
from jax.experimental.pallas import tpu as pltpu
from jax.sharding import PartitionSpec as P


LEN = 64
NZ, NY = 16, 4
BF = jnp.bfloat16
F32 = jnp.float32
VMEM = pl.BlockSpec(memory_space=pltpu.VMEM)
SMEM = pl.BlockSpec(memory_space=pltpu.SMEM)


def limit(mib):
    return pltpu.CompilerParams(vmem_limit_bytes=mib * 1024 * 1024)


OFFSETS = tuple(range(-8, 8))
BATCHES = ((0, -1, 1, -2, 2, -3, 3, -4, 4, -5, 5), (-6, 6, -7, 7, -8))
HBM = pl.BlockSpec(memory_space=pltpu.HBM)


def fs_shift(dy, dz):
    return [
        (z * NY + y, ((z + dz) % NZ) * NY + (y + dy) % NY) for z in range(NZ) for y in range(NY)
    ]


def shift(array, dy=0, dz=0):
    return lax.ppermute(array, "fs", fs_shift(dy, dz))


def rolled(array, first_block):
    twice = jnp.concatenate([array, array], axis=1)
    return lax.dynamic_slice_in_dim(twice, first_block * 128, array.shape[1], 1)


def pack_kernel(gate_in, up_in, mix_in, mix_out, down_in, first_ref, second_ref, *scratch):
    held, sems = scratch[:5], scratch[5]
    copies = []
    for k, (src, dst) in enumerate(zip((gate_in, up_in, mix_in, mix_out, down_in), held)):
        copies.append(pltpu.make_async_copy(src, dst, sems.at[k]))
        copies[-1].start()
    for copy in copies:
        copy.wait()
    gate_ref, up_ref, in_ref, out_ref, down_ref = held
    width = gate_ref.shape[1]
    whole = width // 128 * 128
    first_ref[:, :whole] = gate_ref[:, :whole]
    first_ref[:, whole : 2 * whole] = up_ref[:, :whole]
    first_ref[:, 2 * whole :] = jnp.concatenate([gate_ref[:, whole:], up_ref[:, whole:]], axis=1)
    second_ref[:, 0:128] = in_ref[...]
    second_ref[:, 128:256] = out_ref[...]
    second_ref[:, 256 : 256 + width] = down_ref[...]
    second_ref[:, 256 + width :] = jnp.zeros((32, width - 256), BF)


def pack(*weights):
    shape = jax.ShapeDtypeStruct((32, 2 * weights[0].shape[1]), BF)
    return pl.pallas_call(
        pack_kernel,
        out_shape=(shape, shape),
        in_specs=[HBM] * 5,
        out_specs=(VMEM, VMEM),
        scratch_shapes=[pltpu.VMEM(w.shape, BF) for w in weights] + [pltpu.SemaphoreType.DMA((5,))],
        compiler_params=limit(63),
        cost_estimate=pl.CostEstimate(flops=10**8, bytes_accessed=1 << 18, transcendentals=0),
        name="pack",
    )(*weights)


def by_core(core, blocks):
    even, odd = blocks[0::2], blocks[1::2]
    mine = [jnp.where(core == 0, a, b) for a, b in zip(even, odd)]
    other = [jnp.where(core == 0, b, a) for a, b in zip(even, odd)]
    return jnp.concatenate(mine + other, axis=0)


def first_norm_kernel(at_ref, x_ref, gain_ref, out_ref):
    rows, depth = x_ref.shape
    tile = rows // 8
    block, core = at_ref[0], at_ref[1]
    halves = ([], [])
    for i in range(4):
        x0 = x_ref[2 * i * tile : (2 * i + 1) * tile, :].astype(F32)
        x1 = x_ref[(2 * i + 1) * tile : (2 * i + 2) * tile, :].astype(F32)
        for k, x in enumerate((x0, x1)):
            scale = lax.rsqrt(jnp.mean(x * x, axis=-1, keepdims=True) + 1e-06)
            halves[k].append(scale)
    for p in range(depth // 128):
        start = pl.multiple_of(lax.rem(block + p, depth // 128) * 128, 128)
        gain = gain_ref[0:1, p * 128 : (p + 1) * 128]
        mine, other = [], []
        for i in range(4):
            x0 = x_ref[2 * i * tile : (2 * i + 1) * tile, pl.ds(start, 128)].astype(F32)
            x1 = x_ref[(2 * i + 1) * tile : (2 * i + 2) * tile, pl.ds(start, 128)].astype(F32)
            x0 = (x0 * halves[0][i] * gain).astype(BF)
            x1 = (x1 * halves[1][i] * gain).astype(BF)
            mine.append(jnp.where(core == 0, x0, x1))
            other.append(jnp.where(core == 0, x1, x0))
        for i in range(4):
            out_ref[i * tile : (i + 1) * tile, p * 128 : (p + 1) * 128] = mine[i]
            out_ref[(4 + i) * tile : (5 + i) * tile, p * 128 : (p + 1) * 128] = other[i]


def first_norm(at, tokens, gain):
    return pl.pallas_call(
        first_norm_kernel,
        out_shape=jax.ShapeDtypeStruct(tokens.shape, BF),
        in_specs=[SMEM, VMEM, VMEM],
        out_specs=VMEM,
        compiler_params=limit(8),
        cost_estimate=pl.CostEstimate(flops=10**9, bytes_accessed=3 << 20, transcendentals=0),
        name="first_norm",
    )(at, tokens, gain)


def rms_scale(values, gain):
    return values * lax.rsqrt(jnp.mean(values * values, axis=-1, keepdims=True) + 1e-06) * gain


def settle_kernel(factor, parts_ref, stream_ref, gain_ref, next_ref, new_ref, normed_ref):
    total = parts_ref[0].astype(F32)
    for k in range(1, parts_ref.shape[0]):
        total = total + parts_ref[k].astype(F32)
    stream = stream_ref[...] + factor * rms_scale(total, gain_ref[...])
    new_ref[...] = stream
    normed_ref[...] = rms_scale(stream, next_ref[...]).astype(BF)


def settle(parts, stream, gain, next_gain, factor):
    return pl.pallas_call(
        functools.partial(settle_kernel, factor),
        out_shape=(
            jax.ShapeDtypeStruct(stream.shape, F32),
            jax.ShapeDtypeStruct(stream.shape, BF),
        ),
        in_specs=[VMEM] * 4,
        out_specs=(VMEM, VMEM),
        compiler_params=limit(6),
        cost_estimate=pl.CostEstimate(flops=10**8, bytes_accessed=1 << 20, transcendentals=0),
        name="settle",
    )(parts, stream, gain, next_gain)


def finish_kernel(at_ref, parts_ref, stream_ref, gain_ref, out_ref):
    total = parts_ref[0].astype(F32)
    for k in range(1, parts_ref.shape[0]):
        total = total + parts_ref[k].astype(F32)
    result = (stream_ref[...] + 0.5 * rms_scale(total, gain_ref[...])).astype(BF)
    blocks = result.shape[1] // 128
    for p in range(blocks):
        start = pl.multiple_of(lax.rem(at_ref[0] + p, blocks) * 128, 128)
        out_ref[:, pl.ds(start, 128)] = result[:, p * 128 : (p + 1) * 128]


def finish(at, parts, stream, gain):
    return pl.pallas_call(
        finish_kernel,
        out_shape=jax.ShapeDtypeStruct(stream.shape, BF),
        in_specs=[SMEM] + [VMEM] * 3,
        out_specs=VMEM,
        compiler_params=limit(6),
        cost_estimate=pl.CostEstimate(flops=10**8, bytes_accessed=1 << 20, transcendentals=0),
        name="finish",
    )(at, parts, stream, gain)


def gated_kernel(width, parts, *refs):
    payloads, out_ref, w_ref = refs[parts : parts + NZ], refs[-2], refs[-1]
    for k in range(NZ):
        w_ref[k * 128 : (k + 1) * 128, :] = payloads[k][0:128, :]
    x = jnp.concatenate([ref[...] for ref in refs[:parts]], axis=0)
    whole = width // 128 * 128

    def act(gate, up):
        return (gate / (1.0 + jnp.exp(-gate)) * up).astype(BF)

    at = 0
    while at < whole:
        n = min(256, whole - at)
        gate = jnp.dot(x, w_ref[:, at : at + n], preferred_element_type=F32)
        up = jnp.dot(x, w_ref[:, whole + at : whole + at + n], preferred_element_type=F32)
        out_ref[:, at : at + n] = act(gate, up)
        at += n
    if width > whole:
        rest = width - whole
        both = jnp.dot(x, w_ref[:, 2 * whole :], preferred_element_type=F32)
        out_ref[:, whole:] = act(both[:, :rest], both[:, rest:])


def gated(xs, payloads, width):
    rows, depth = sum(x.shape[0] for x in xs), xs[0].shape[1]
    return pl.pallas_call(
        functools.partial(gated_kernel, width, len(xs)),
        out_shape=jax.ShapeDtypeStruct((rows, width), BF),
        in_specs=[VMEM] * (len(xs) + NZ),
        out_specs=VMEM,
        scratch_shapes=[pltpu.VMEM((depth, 2 * width), BF)],
        compiler_params=limit(24),
        cost_estimate=pl.CostEstimate(
            flops=4 * rows * depth * width, bytes_accessed=8 << 20, transcendentals=0
        ),
        name="gated",
    )(*xs, *payloads)


def assemble_kernel(batch, y_ref, *refs):
    ins, mix_ref, down_ref = refs[:NY], refs[-2], refs[-1]
    y = y_ref[0]
    width = mix_ref.shape[1] + down_ref.shape[1]
    for j in range(NY):
        owner = lax.rem(y - j + NY, NY)
        for i, offset in enumerate(batch):
            start = pl.multiple_of(OFFSETS.index(offset) * 128 + owner * 32, 32)
            mix_ref[pl.ds(start, 32), :] = ins[j][i * 32 : (i + 1) * 32, 0:256]
            down_ref[pl.ds(start, 32), :] = ins[j][i * 32 : (i + 1) * 32, 256:width]


def assemble(y, pieces, batch, down_width, before=()):
    rows = NZ * NY * 32
    return pl.pallas_call(
        functools.partial(assemble_kernel, batch),
        out_shape=(
            jax.ShapeDtypeStruct((rows, 256), BF),
            jax.ShapeDtypeStruct((rows, down_width), BF),
        ),
        in_specs=[SMEM] + [VMEM] * (NY + len(before)),
        out_specs=(VMEM, VMEM),
        input_output_aliases={1 + NY: 0, 2 + NY: 1} if before else {},
        compiler_params=limit(12),
        cost_estimate=pl.CostEstimate(flops=10**8, bytes_accessed=8 << 20, transcendentals=0),
        name="assemble",
    )(y, *pieces, *before)


def down_kernel(h_ref, w_ref, mine_ref, other_ref):
    h = h_ref[...]
    half = h.shape[0] // 2
    for at in range(0, w_ref.shape[0], 256):
        share = lax.dot_general(
            h, w_ref[at : at + 256, :], (((1,), (1,)), ((), ())), preferred_element_type=F32
        ).astype(BF)
        mine_ref[:, at : at + 256] = share[:half]
        other_ref[:, at : at + 256] = share[half:]


def down(hidden, w):
    rows, out = hidden.shape[0], w.shape[0]
    return pl.pallas_call(
        down_kernel,
        out_shape=(jax.ShapeDtypeStruct((rows // 2, out), BF),) * 2,
        in_specs=[VMEM, VMEM],
        out_specs=(VMEM, VMEM),
        compiler_params=limit(14),
        cost_estimate=pl.CostEstimate(
            flops=2 * rows * out * w.shape[1], bytes_accessed=4 << 20, transcendentals=0
        ),
        name="down",
    )(hidden, w)


def mixer_kernel(kind_ref, mine_ref, other_ref, w_ref, pool_ref, scale_ref, keep_ref, send_ref):
    rows = 2 * mine_ref.shape[0]
    tile = rows // 8
    kind, core = kind_ref[0], kind_ref[1]
    x = jnp.concatenate([mine_ref[...], other_ref[...]], axis=0)
    values = jnp.dot(x, w_ref[:, 0:128], preferred_element_type=F32)
    values = values.astype(BF).astype(F32)
    in_order = []
    for i in range(4):
        mine = values[i * tile : (i + 1) * tile]
        other = values[(4 + i) * tile : (5 + i) * tile]
        in_order += [jnp.where(core == 0, mine, other), jnp.where(core == 0, other, mine)]
    values = jnp.concatenate(in_order, axis=0)
    place = lax.broadcasted_iota(jnp.int32, (rows, 128), 0) % LEN
    total = values
    chosen = jnp.zeros_like(values)
    for slot in range(4):
        lag = 2**slot
        earlier = jnp.concatenate([jnp.zeros((lag, 128), F32), total[: rows - lag]], axis=0)
        total = total + jnp.where(place >= lag, earlier, 0.0)
        window = 2 * lag
        mean = total / jnp.minimum(place + 1, window).astype(F32)
        chosen = jnp.where(kind == slot, mean, chosen)
    deviation = (chosen - values).astype(BF)
    mixed = jnp.dot(deviation, pool_ref[...], preferred_element_type=F32)
    mixed = mixed * scale_ref[...].astype(F32)
    mixed = by_core(core, [mixed[i * tile : (i + 1) * tile] for i in range(8)]).astype(BF)
    for at in range(0, w_ref.shape[0], 256):
        share = lax.dot_general(
            mixed, w_ref[at : at + 256, 128:256], (((1,), (1,)), ((), ())), preferred_element_type=F32
        ).astype(BF)
        keep_ref[:, at : at + 256] = share[: rows // 2]
        send_ref[:, at : at + 256] = share[rows // 2 :]


def mixer(kind, mine, other, w, pool_w, pool_scale):
    rows, depth = 2 * mine.shape[0], mine.shape[1]
    return pl.pallas_call(
        mixer_kernel,
        out_shape=(jax.ShapeDtypeStruct((rows // 2, depth), BF),) * 2,
        in_specs=[SMEM] + [VMEM] * 5,
        out_specs=(VMEM, VMEM),
        compiler_params=limit(14),
        cost_estimate=pl.CostEstimate(
            flops=4 * rows * depth * 128, bytes_accessed=4 << 20, transcendentals=0
        ),
        name="mixer",
    )(kind, mine, other, w, pool_w, pool_scale)


X_GROUPS = [[2 * x + core for x in range(4)] for core in range(2)]


def core_swap(array):
    return lax.ppermute(array, "tp", [(k, k ^ 1) for k in range(8)])


def shares_of_rows(mine, other):
    both = (mine.astype(F32) + core_swap(other).astype(F32)).astype(BF)
    tiles = both.reshape(4, both.shape[0] // 4, both.shape[1])
    return lax.all_to_all(tiles, "tp", 0, 0, tiled=True, axis_index_groups=X_GROUPS)


def rows_of_all(normed):
    mine = lax.all_gather(normed, "tp", axis=0, tiled=True, axis_index_groups=X_GROUPS)
    return mine, core_swap(mine)


def body(tokens, w_gate, w_up, w_down, w_mix_in, w_mix_out, pool_w, pool_scale, norm_gains):
    tp_size, tp_at = lax.axis_size("tp"), lax.axis_index("tp")
    fs_at = lax.axis_index("fs")
    z, y = fs_at // NY, fs_at % NY
    own_rows = tokens.shape[0] // tp_size
    width = w_gate.shape[1]

    groups = [[k * NY + j for j in range(NY)] for k in range(NZ)]
    second_width = 256 + width
    first, second = pack(w_gate, w_up, w_mix_in, w_mix_out.T, w_down.T)
    first = lax.all_gather(first, "fs", axis=0, tiled=True, axis_index_groups=groups)

    first_block = lax.rem(z + 8, NZ)
    core = lax.rem(tp_at, 2)
    gains = rolled(norm_gains, first_block)
    gain = [gains[k : k + 1] for k in range(6)]
    numbers = jnp.stack([first_block, core, lax.rem(tp_at, 4), y]).astype(jnp.int32)

    back = ahead = jnp.concatenate([first, second], axis=0)
    got = {0: back}
    for k in range(1, 9):
        if k == 7:
            last_second = shift(back[128:, :second_width], dz=2)
        back = got[-k] = shift(back if k < 8 else back[:128], dz=1)
        if k < 8:
            ahead = got[k] = shift(ahead, dz=-1)
        if k == 2:
            back, late_tokens = lax.optimization_barrier((back, tokens))
            x = first_norm(numbers[0:2], late_tokens, gain[0])
        if k == 5:
            back, x = lax.optimization_barrier((back, x))
        got[-k] = back
    payloads = [got[k] for k in OFFSETS]

    late = ()
    for batch in BATCHES:
        own = [last_second if s == -8 else got[s][128:, :second_width] for s in batch]
        own = jnp.concatenate(own, axis=0)
        pieces = [own, shift(own, dy=1), shift(own, dy=2), shift(own, dy=-1)]
        late = assemble(numbers[3:4], pieces, batch, width, late)
    mix_w, down_w = late

    stream = lax.dynamic_slice_in_dim(tokens, tp_at * own_rows, own_rows, 0)
    stream = rolled(stream, first_block).astype(F32)
    parts = shares_of_rows(*down(gated([x], payloads, width), down_w))
    stream, normed = settle(parts, stream, gain[1], gain[2], 0.5)
    kind = jnp.stack([numbers[2], numbers[1]])
    share = mixer(kind, *rows_of_all(normed), mix_w, pool_w[0], pool_scale[None])
    stream, normed = settle(shares_of_rows(*share), stream, gain[3], gain[4], 1.0)
    hidden = gated(rows_of_all(normed), payloads, width)
    parts = shares_of_rows(*down(hidden, down_w))
    return finish(numbers[0:1], parts, stream, gain[5])


def solution(mesh):
    in_specs = (
        P("fs", None),
        P("fs", "tp"),
        P("fs", "tp"),
        P("tp", "fs"),
        P("fs", "tp"),
        P("tp", "fs"),
        P("tp", None, None),
        P("tp"),
        P(),
    )
    out_specs = P(("fs", "tp"), None)

    return jax.shard_map(body, mesh=mesh, in_specs=in_specs, out_specs=out_specs, check_vma=False)
```

profile of v0, /device:TPU:1, one launch (start us, length us, event | category | flops | bytes accessed | tf_op | source)
XLA Modules:
  0.0 266.4 jit_solution(13337339015918783403)
XLA Ops:
  1.7 11.2 %all_gather.9 = bf16[128,1408]{1,0:T(8,128)(2,1)S(1)} all-gather(bf16[32,1408]{1,0:T(8,128)(2,1)} %get-tuple-element.25), channel_id=1, replica_groups={{0,8,16,24},{32,40,48,56},{64,72,80,88},{96,104,112,120},{128,136,144,1..., dimensions={0}, use_global_device_ids=true | all-gather | bytes 450560 | tf_op jit(solution)/shard_map/all_gather | solution.py:346
  13.9 4.5 %collective-permute-start = (bf16[160,1408]{1,0:T(8,128)(2,1)S(1)}, bf16[160,1408]{1,0:T(8,128)(2,1)S(1)}, u32[]{:S(2)}, u32[]{:S(2)}) collective-permute-start(bf16[160,1408]{1,0:T(8,128)(2,1)S(1)} %constant_dynamic-update-slice_fusion.refs_9_.refs_10_), channel_id=1, source_target_pairs={{0,32},{8,40},{16,48},{24,56},{32,64},{40,72},{48,80},{56,88},{64,... | collective-permute-start | bytes 1351688 | tf_op jit(solution)/shard_map/ppermute | solution.py:35
  18.4 9.5 %collective-permute-start.8 = (bf16[160,1408]{1,0:T(8,128)(2,1)S(1)}, bf16[160,1408]{1,0:T(8,128)(2,1)S(1)}, u32[]{:S(2)}, u32[]{:S(2)}) collective-permute-start(bf16[160,1408]{1,0:T(8,128)(2,1)S(1)} %constant_dynamic-update-slice_fusion.refs_9_.refs_10_), channel_id=1, source_target_pairs={{0,480},{8,488},{16,496},{24,504},{32,0},{40,8},{48,16},{56,24},{6... | collective-permute-start | bytes 1351688 | tf_op jit(solution)/shard_map/ppermute | solution.py:35
  28.8 5.4 %collective-permute-done.refs_8_.refs_9_ = bf16[160,1408]{1,0:T(8,128)(2,1)S(1)} collective-permute-done((bf16[160,1408]{1,0:T(8,128)(2,1)S(1)}, bf16[160,1408]{1,0:T(8,128)(2,1)S(1)}, u32[]{:S(2)}, u32[]{:S(2)}) %collective-permute-start) | collective-permute-done | bytes 450592 | tf_op jit(solution)/shard_map/ppermute | solution.py:35
  36.1 4.6 %collective-permute-start.9 = (bf16[160,1408]{1,0:T(8,128)(2,1)S(1)}, bf16[160,1408]{1,0:T(8,128)(2,1)S(1)}, u32[]{:S(2)}, u32[]{:S(2)}) collective-permute-start(bf16[160,1408]{1,0:T(8,128)(2,1)S(1)} %collective-permute-done.8.refs_10_.refs_11_), channel_id=1, source_target_pairs={{0,480},{8,488},{16,496},{24,504},{32,0},{40,8},{48,16},{56,24},{6... | collective-permute-start | bytes 1351688 | tf_op jit(solution)/shard_map/ppermute | solution.py:35
  40.7 5.3 %collective-permute-done.1.refs_7_.refs_8_ = bf16[160,1408]{1,0:T(8,128)(2,1)S(1)} collective-permute-done((bf16[160,1408]{1,0:T(8,128)(2,1)S(1)}, bf16[160,1408]{1,0:T(8,128)(2,1)S(1)}, u32[]{:S(2)}, u32[]{:S(2)}) %collective-permute-start.1) | collective-permute-done | bytes 450592 | tf_op jit(solution)/shard_map/ppermute | solution.py:35
  50.4 4.6 %collective-permute-start.10 = (bf16[160,1408]{1,0:T(8,128)(2,1)S(1)}, bf16[160,1408]{1,0:T(8,128)(2,1)S(1)}, u32[]{:S(2)}, u32[]{:S(2)}) collective-permute-start(bf16[160,1408]{1,0:T(8,128)(2,1)S(1)} %collective-permute-done.9.refs_11_.refs_12_), channel_id=1, source_target_pairs={{0,480},{8,488},{16,496},{24,504},{32,0},{40,8},{48,16},{56,24},{6... | collective-permute-start | bytes 1351688 | tf_op jit(solution)/shard_map/ppermute | solution.py:35
  60.3 5.4 %collective-permute-start.11 = (bf16[160,1408]{1,0:T(8,128)(2,1)S(1)}, bf16[160,1408]{1,0:T(8,128)(2,1)S(1)}, u32[]{:S(2)}, u32[]{:S(2)}) collective-permute-start(bf16[160,1408]{1,0:T(8,128)(2,1)S(1)} %collective-permute-done.10.refs_12_.refs_13_), channel_id=1, source_target_pairs={{0,480},{8,488},{16,496},{24,504},{32,0},{40,8},{48,16},{56,24},{6... | collective-permute-start | bytes 1351688 | tf_op jit(solution)/shard_map/ppermute | solution.py:35
  71.0 5.0 %collective-permute-start.12 = (bf16[160,1408]{1,0:T(8,128)(2,1)S(1)}, bf16[160,1408]{1,0:T(8,128)(2,1)S(1)}, u32[]{:S(2)}, u32[]{:S(2)}) collective-permute-start(bf16[160,1408]{1,0:T(8,128)(2,1)S(1)} %collective-permute-done.11.refs_13_.refs_14_), channel_id=1, source_target_pairs={{0,480},{8,488},{16,496},{24,504},{32,0},{40,8},{48,16},{56,24},{6... | collective-permute-start | bytes 1351688 | tf_op jit(solution)/shard_map/ppermute | solution.py:35
  81.4 5.0 %collective-permute-start.13 = (bf16[160,1408]{1,0:T(8,128)(2,1)S(1)}, bf16[160,1408]{1,0:T(8,128)(2,1)S(1)}, u32[]{:S(2)}, u32[]{:S(2)}) collective-permute-start(bf16[160,1408]{1,0:T(8,128)(2,1)S(1)} %collective-permute-done.12.refs_14_.refs_15_), channel_id=1, source_target_pairs={{0,480},{8,488},{16,496},{24,504},{32,0},{40,8},{48,16},{56,24},{6... | collective-permute-start | bytes 1351688 | tf_op jit(solution)/shard_map/ppermute | solution.py:35
  89.2 3.9 %collective-permute-start.20 = (bf16[352,960]{1,0:T(8,128)(2,1)S(1)}, bf16[352,960]{1,0:T(8,128)(2,1)S(1)}, u32[]{:S(2)}, u32[]{:S(2)}) collective-permute-start(bf16[352,960]{1,0:T(8,128)(2,1)S(1)} %slice_dynamic-update-slice_fusion.refs_0_), channel_id=1, source_target_pairs={{0,16},{8,24},{16,0},{24,8},{32,48},{40,56},{48,32},{56,40},{64,80... | collective-permute-start | bytes 2027528 | tf_op jit(solution)/shard_map/ppermute | solution.py:35
  93.1 3.2 %collective-permute-start.21 = (bf16[352,960]{1,0:T(8,128)(2,1)S(1)}, bf16[352,960]{1,0:T(8,128)(2,1)S(1)}, u32[]{:S(2)}, u32[]{:S(2)}) collective-permute-start(bf16[352,960]{1,0:T(8,128)(2,1)S(1)} %slice_dynamic-update-slice_fusion.refs_0_), channel_id=1, source_target_pairs={{0,24},{8,0},{16,8},{24,16},{32,56},{40,32},{48,40},{56,48},{64,88... | collective-permute-start | bytes 2027528 | tf_op jit(solution)/shard_map/ppermute | solution.py:35
  99.1 4.6 %collective-permute-start.14 = (bf16[160,1408]{1,0:T(8,128)(2,1)S(1)}, bf16[160,1408]{1,0:T(8,128)(2,1)S(1)}, u32[]{:S(2)}, u32[]{:S(2)}) collective-permute-start(bf16[160,1408]{1,0:T(8,128)(2,1)S(1)} %collective-permute-done.13.refs_15_.refs_16_), channel_id=1, source_target_pairs={{0,480},{8,488},{16,496},{24,504},{32,0},{40,8},{48,16},{56,24},{6... | collective-permute-start | bytes 1351688 | tf_op jit(solution)/shard_map/ppermute | solution.py:35
  123.3 4.0 %collective-permute-start.18 = (bf16[160,960]{1,0:T(8,128)(2,1)}, bf16[160,960]{1,0:T(8,128)(2,1)}, u32[]{:S(2)}, u32[]{:S(2)}) collective-permute-start(bf16[160,960]{1,0:T(8,128)(2,1)} %constant_dynamic-update-slice_fusion.2.refs_0_), channel_id=1, source_target_pairs={{0,24},{8,0},{16,8},{24,16},{32,56},{40,32},{48,40},{56,48},{64,88... | collective-permute-start | bytes 921608 | tf_op jit(solution)/shard_map/ppermute | solution.py:35
  140.8 20.2 %collective-permute-start.22 = (bf16[160,2048]{1,0:T(8,128)(2,1)S(1)}, bf16[160,2048]{1,0:T(8,128)(2,1)S(1)}, u32[]{:S(2)}, u32[]{:S(2)}) collective-permute-start(bf16[160,2048]{1,0:T(8,128)(2,1)S(1)} %get-tuple-element.35), channel_id=1, source_target_pairs={{0,1},{1,0},{2,3},{3,2},{4,5},{5,4},{6,7},{7,6},{8,9},{9,8},{10,11... | collective-permute-start | bytes 1966088 | tf_op jit(solution)/shard_map/ppermute | solution.py:322
  163.8 4.2 %all-to-all-start = ((bf16[4,40,2048]{2,1,0:T(8,128)(2,1)}), bf16[4,40,2048]{2,1,0:T(8,128)(2,1)}, u32[]{:S(2)}, u32[]{:S(2)}) async-start(bf16[4,40,2048]{2,1,0:T(8,128)(2,1)} %bitcast.13), calls=%async_computation | async-start | bytes 1310720 | tf_op jit(solution)/shard_map/all_to_all | solution.py:328
  169.7 8.7 %all-to-all-done.parts_ref = bf16[4,40,2048]{2,1,0:T(8,128)(2,1)} async-done(((bf16[4,40,2048]{2,1,0:T(8,128)(2,1)}), bf16[4,40,2048]{2,1,0:T(8,128)(2,1)}, u32[]{:S(2)}, u32[]{:S(2)}) %all-to-all-start) | async-done | bytes 655392 | tf_op jit(solution)/shard_map/all_to_all | solution.py:328
  182.9 11.2 %all_gather.10.mine_ref = bf16[160,2048]{1,0:T(8,128)(2,1)} all-gather(bf16[40,2048]{1,0:T(8,128)(2,1)S(1)} %get-tuple-element.36), channel_id=1, replica_groups={{0,2,4,6},{1,3,5,7},{8,10,12,14},{9,11,13,15},{16,18,20,22},{17,19,21,2..., dimensions={0}, use_global_device_ids=true | all-gather | bytes 819200 | tf_op jit(solution)/shard_map/all_gather | solution.py:332
  194.1 6.6 %collective-permute-start.23 = (bf16[160,2048]{1,0:T(8,128)(2,1)}, bf16[160,2048]{1,0:T(8,128)(2,1)}, u32[]{:S(2)}, u32[]{:S(2)}) collective-permute-start(bf16[160,2048]{1,0:T(8,128)(2,1)} %all_gather.10.mine_ref), channel_id=1, source_target_pairs={{0,1},{1,0},{2,3},{3,2},{4,5},{5,4},{6,7},{7,6},{8,9},{9,8},{10,11... | collective-permute-start | bytes 1966088 | tf_op jit(solution)/shard_map/ppermute | solution.py:322
  204.7 3.2 %mixer.1 = (bf16[160,2048]{1,0:T(8,128)(2,1)S(1)}, bf16[160,2048]{1,0:T(8,128)(2,1)S(1)}) custom-call(s32[2]{0:T(128)S(1)} %pad_add_fusion.kind_ref, bf16[160,2048]{1,0:T(8,128)(2,1)} %all_gather.10.mine_ref, bf16[160,2048]{1,0:T(8,128)(2,1)} %collective-permute-done.23.other_ref, bf16[2048,256]{1,0:T(8,128)(2,1)S(1)} %copy-done.1, ...), custom_call_target="tpu_custom_call" | custom-call | flops 335544320 | bytes 4194304 | tf_op jit(solution)/shard_map/mixer/pallas_call | solution.py:305
  212.2 13.1 %all_to_all.15.parts_ref = bf16[4,40,2048]{2,1,0:T(8,128)(2,1)S(1)} all-to-all(bf16[4,40,2048]{2,1,0:T(8,128)(2,1)S(1)} %bitcast.14), channel_id=1, replica_groups={{0,2,4,6},{1,3,5,7},{8,10,12,14},{9,11,13,15},{16,18,20,22},{17,19,21,2..., dimensions={0} | all-to-all | bytes 1310720 | tf_op jit(solution)/shard_map/all_to_all | solution.py:328
  225.7 10.8 %all_gather.11.refs_0_ = bf16[160,2048]{1,0:T(8,128)(2,1)S(1)} all-gather(bf16[40,2048]{1,0:T(8,128)(2,1)S(1)} %get-tuple-element.41), channel_id=1, replica_groups={{0,2,4,6},{1,3,5,7},{8,10,12,14},{9,11,13,15},{16,18,20,22},{17,19,21,2..., dimensions={0}, use_global_device_ids=true | all-gather | bytes 819200 | tf_op jit(solution)/shard_map/all_gather | solution.py:332
  236.4 6.5 %collective-permute-start.25 = (bf16[160,2048]{1,0:T(8,128)(2,1)S(1)}, bf16[160,2048]{1,0:T(8,128)(2,1)S(1)}, u32[]{:S(2)}, u32[]{:S(2)}) collective-permute-start(bf16[160,2048]{1,0:T(8,128)(2,1)S(1)} %all_gather.11.refs_0_), channel_id=1, source_target_pairs={{0,1},{1,0},{2,3},{3,2},{4,5},{5,4},{6,7},{7,6},{8,9},{9,8},{10,11... | collective-permute-start | bytes 1966088 | tf_op jit(solution)/shard_map/ppermute | solution.py:322
  252.7 12.9 %all_to_all.16.parts_ref = bf16[4,40,2048]{2,1,0:T(8,128)(2,1)S(1)} all-to-all(bf16[4,40,2048]{2,1,0:T(8,128)(2,1)S(1)} %bitcast.15), channel_id=1, replica_groups={{0,2,4,6},{1,3,5,7},{8,10,12,14},{9,11,13,15},{16,18,20,22},{17,19,21,2..., dimensions={0} | all-to-all | bytes 1310720 | tf_op jit(solution)/shard_map/all_to_all | solution.py:328
  (213 shorter events, 91.9 us)
Async XLA Ops:
  13.9 20.2 %collective-permute-start = (bf16[160,1408]{1,0:T(8,128)(2,1)S(1)}, bf16[160,1408]{1,0:T(8,128)(2,1)S(1)}, u32[]{:S(2)}, u32[]{:S(2)}) collective-permute-start(bf16[160,1408]{1,0:T(8,128)(2,1)S(1)} %constant_dynamic-update-slice_fusion.refs_9_.refs_10_), channel_id=1, source_target_pairs={{0,32},{8,40},{16,48},{24,56},{32,64},{40,72},{48,80},{56,88},{64,... | collective-permute-start | bytes 1351688 | tf_op jit(solution)/shard_map/ppermute | solution.py:35
  18.4 17.6 %collective-permute-start.8 = (bf16[160,1408]{1,0:T(8,128)(2,1)S(1)}, bf16[160,1408]{1,0:T(8,128)(2,1)S(1)}, u32[]{:S(2)}, u32[]{:S(2)}) collective-permute-start(bf16[160,1408]{1,0:T(8,128)(2,1)S(1)} %constant_dynamic-update-slice_fusion.refs_9_.refs_10_), channel_id=1, source_target_pairs={{0,480},{8,488},{16,496},{24,504},{32,0},{40,8},{48,16},{56,24},{6... | collective-permute-start | bytes 1351688 | tf_op jit(solution)/shard_map/ppermute | solution.py:35
  34.1 11.8 %collective-permute-start.1 = (bf16[160,1408]{1,0:T(8,128)(2,1)S(1)}, bf16[160,1408]{1,0:T(8,128)(2,1)S(1)}, u32[]{:S(2)}, u32[]{:S(2)}) collective-permute-start(bf16[160,1408]{1,0:T(8,128)(2,1)S(1)} %collective-permute-done.refs_8_.refs_9_), channel_id=1, source_target_pairs={{0,32},{8,40},{16,48},{24,56},{32,64},{40,72},{48,80},{56,88},{64,... | collective-permute-start | bytes 1351688 | tf_op jit(solution)/shard_map/ppermute | solution.py:35
  36.1 14.3 %collective-permute-start.9 = (bf16[160,1408]{1,0:T(8,128)(2,1)S(1)}, bf16[160,1408]{1,0:T(8,128)(2,1)S(1)}, u32[]{:S(2)}, u32[]{:S(2)}) collective-permute-start(bf16[160,1408]{1,0:T(8,128)(2,1)S(1)} %collective-permute-done.8.refs_10_.refs_11_), channel_id=1, source_target_pairs={{0,480},{8,488},{16,496},{24,504},{32,0},{40,8},{48,16},{56,24},{6... | collective-permute-start | bytes 1351688 | tf_op jit(solution)/shard_map/ppermute | solution.py:35
  46.0 11.0 %collective-permute-start.2 = (bf16[160,1408]{1,0:T(8,128)(2,1)S(1)}, bf16[160,1408]{1,0:T(8,128)(2,1)S(1)}, u32[]{:S(2)}, u32[]{:S(2)}) collective-permute-start(bf16[160,1408]{1,0:T(8,128)(2,1)S(1)} %collective-permute-done.1.refs_7_.refs_8_), channel_id=1, source_target_pairs={{0,32},{8,40},{16,48},{24,56},{32,64},{40,72},{48,80},{56,88},{64,... | collective-permute-start | bytes 1351688 | tf_op jit(solution)/shard_map/ppermute | solution.py:35
  50.4 9.9 %collective-permute-start.10 = (bf16[160,1408]{1,0:T(8,128)(2,1)S(1)}, bf16[160,1408]{1,0:T(8,128)(2,1)S(1)}, u32[]{:S(2)}, u32[]{:S(2)}) collective-permute-start(bf16[160,1408]{1,0:T(8,128)(2,1)S(1)} %collective-permute-done.9.refs_11_.refs_12_), channel_id=1, source_target_pairs={{0,480},{8,488},{16,496},{24,504},{32,0},{40,8},{48,16},{56,24},{6... | collective-permute-start | bytes 1351688 | tf_op jit(solution)/shard_map/ppermute | solution.py:35
  57.0 10.3 %collective-permute-start.3 = (bf16[160,1408]{1,0:T(8,128)(2,1)S(1)}, bf16[160,1408]{1,0:T(8,128)(2,1)S(1)}, u32[]{:S(2)}, u32[]{:S(2)}) collective-permute-start(bf16[160,1408]{1,0:T(8,128)(2,1)S(1)} %collective-permute-done.2.refs_6_.refs_7_), channel_id=1, source_target_pairs={{0,32},{8,40},{16,48},{24,56},{32,64},{40,72},{48,80},{56,88},{64,... | collective-permute-start | bytes 1351688 | tf_op jit(solution)/shard_map/ppermute | solution.py:35
  60.3 10.7 %collective-permute-start.11 = (bf16[160,1408]{1,0:T(8,128)(2,1)S(1)}, bf16[160,1408]{1,0:T(8,128)(2,1)S(1)}, u32[]{:S(2)}, u32[]{:S(2)}) collective-permute-start(bf16[160,1408]{1,0:T(8,128)(2,1)S(1)} %collective-permute-done.10.refs_12_.refs_13_), channel_id=1, source_target_pairs={{0,480},{8,488},{16,496},{24,504},{32,0},{40,8},{48,16},{56,24},{6... | collective-permute-start | bytes 1351688 | tf_op jit(solution)/shard_map/ppermute | solution.py:35
  67.3 10.3 %collective-permute-start.4 = (bf16[160,1408]{1,0:T(8,128)(2,1)S(1)}, bf16[160,1408]{1,0:T(8,128)(2,1)S(1)}, u32[]{:S(2)}, u32[]{:S(2)}) collective-permute-start(bf16[160,1408]{1,0:T(8,128)(2,1)S(1)} %collective-permute-done.3.refs_5_.refs_6_), channel_id=1, source_target_pairs={{0,32},{8,40},{16,48},{24,56},{32,64},{40,72},{48,80},{56,88},{64,... | collective-permute-start | bytes 1351688 | tf_op jit(solution)/shard_map/ppermute | solution.py:35
  71.0 10.4 %collective-permute-start.12 = (bf16[160,1408]{1,0:T(8,128)(2,1)S(1)}, bf16[160,1408]{1,0:T(8,128)(2,1)S(1)}, u32[]{:S(2)}, u32[]{:S(2)}) collective-permute-start(bf16[160,1408]{1,0:T(8,128)(2,1)S(1)} %collective-permute-done.11.refs_13_.refs_14_), channel_id=1, source_target_pairs={{0,480},{8,488},{16,496},{24,504},{32,0},{40,8},{48,16},{56,24},{6... | collective-permute-start | bytes 1351688 | tf_op jit(solution)/shard_map/ppermute | solution.py:35
  77.6 19.5 %collective-permute-start.5 = (bf16[160,1408]{1,0:T(8,128)(2,1)S(1)}, bf16[160,1408]{1,0:T(8,128)(2,1)S(1)}, u32[]{:S(2)}, u32[]{:S(2)}) collective-permute-start(bf16[160,1408]{1,0:T(8,128)(2,1)S(1)} %collective-permute-done.4.refs_4_.refs_5_), channel_id=1, source_target_pairs={{0,32},{8,40},{16,48},{24,56},{32,64},{40,72},{48,80},{56,88},{64,... | collective-permute-start | bytes 1351688 | tf_op jit(solution)/shard_map/ppermute | solution.py:35
  81.4 17.6 %collective-permute-start.13 = (bf16[160,1408]{1,0:T(8,128)(2,1)S(1)}, bf16[160,1408]{1,0:T(8,128)(2,1)S(1)}, u32[]{:S(2)}, u32[]{:S(2)}) collective-permute-start(bf16[160,1408]{1,0:T(8,128)(2,1)S(1)} %collective-permute-done.12.refs_14_.refs_15_), channel_id=1, source_target_pairs={{0,480},{8,488},{16,496},{24,504},{32,0},{40,8},{48,16},{56,24},{6... | collective-permute-start | bytes 1351688 | tf_op jit(solution)/shard_map/ppermute | solution.py:35
  87.3 31.1 %collective-permute-start.19 = (bf16[352,960]{1,0:T(8,128)(2,1)S(1)}, bf16[352,960]{1,0:T(8,128)(2,1)S(1)}, u32[]{:S(2)}, u32[]{:S(2)}) collective-permute-start(bf16[352,960]{1,0:T(8,128)(2,1)S(1)} %slice_dynamic-update-slice_fusion.refs_0_), channel_id=1, source_target_pairs={{0,8},{8,16},{16,24},{24,0},{32,40},{40,48},{48,56},{56,32},{64,72... | collective-permute-start | bytes 2027528 | tf_op jit(solution)/shard_map/ppermute | solution.py:35
  89.2 33.2 %collective-permute-start.20 = (bf16[352,960]{1,0:T(8,128)(2,1)S(1)}, bf16[352,960]{1,0:T(8,128)(2,1)S(1)}, u32[]{:S(2)}, u32[]{:S(2)}) collective-permute-start(bf16[352,960]{1,0:T(8,128)(2,1)S(1)} %slice_dynamic-update-slice_fusion.refs_0_), channel_id=1, source_target_pairs={{0,16},{8,24},{16,0},{24,8},{32,48},{40,56},{48,32},{56,40},{64,80... | collective-permute-start | bytes 2027528 | tf_op jit(solution)/shard_map/ppermute | solution.py:35
  93.1 34.2 %collective-permute-start.21 = (bf16[352,960]{1,0:T(8,128)(2,1)S(1)}, bf16[352,960]{1,0:T(8,128)(2,1)S(1)}, u32[]{:S(2)}, u32[]{:S(2)}) collective-permute-start(bf16[352,960]{1,0:T(8,128)(2,1)S(1)} %slice_dynamic-update-slice_fusion.refs_0_), channel_id=1, source_target_pairs={{0,24},{8,0},{16,8},{24,16},{32,56},{40,32},{48,40},{56,48},{64,88... | collective-permute-start | bytes 2027528 | tf_op jit(solution)/shard_map/ppermute | solution.py:35
  97.1 10.6 %collective-permute-start.6 = (bf16[160,1408]{1,0:T(8,128)(2,1)S(1)}, bf16[160,1408]{1,0:T(8,128)(2,1)S(1)}, u32[]{:S(2)}, u32[]{:S(2)}) collective-permute-start(bf16[160,1408]{1,0:T(8,128)(2,1)S(1)} %collective-permute-done.5.refs_3_.refs_4_), channel_id=1, source_target_pairs={{0,32},{8,40},{16,48},{24,56},{32,64},{40,72},{48,80},{56,88},{64,... | collective-permute-start | bytes 1351688 | tf_op jit(solution)/shard_map/ppermute | solution.py:35
  99.1 12.8 %collective-permute-start.14 = (bf16[160,1408]{1,0:T(8,128)(2,1)S(1)}, bf16[160,1408]{1,0:T(8,128)(2,1)S(1)}, u32[]{:S(2)}, u32[]{:S(2)}) collective-permute-start(bf16[160,1408]{1,0:T(8,128)(2,1)S(1)} %collective-permute-done.13.refs_15_.refs_16_), channel_id=1, source_target_pairs={{0,480},{8,488},{16,496},{24,504},{32,0},{40,8},{48,16},{56,24},{6... | collective-permute-start | bytes 1351688 | tf_op jit(solution)/shard_map/ppermute | solution.py:35
  111.9 24.1 %collective-permute-start.7 = (bf16[128,1408]{1,0:T(8,128)(2,1)}, bf16[128,1408]{1,0:T(8,128)(2,1)S(1)}, u32[]{:S(2)}, u32[]{:S(2)}) collective-permute-start(bf16[128,1408]{1,0:T(8,128)(2,1)} %slice.90), channel_id=1, source_target_pairs={{0,32},{8,40},{16,48},{24,56},{32,64},{40,72},{48,80},{56,88},{64,... | collective-permute-start | bytes 1081352 | tf_op jit(solution)/shard_map/ppermute | solution.py:35
  116.5 16.3 %collective-permute-start.16 = (bf16[160,960]{1,0:T(8,128)(2,1)}, bf16[160,960]{1,0:T(8,128)(2,1)}, u32[]{:S(2)}, u32[]{:S(2)}) collective-permute-start(bf16[160,960]{1,0:T(8,128)(2,1)} %constant_dynamic-update-slice_fusion.2.refs_0_), channel_id=1, source_target_pairs={{0,8},{8,16},{16,24},{24,0},{32,40},{40,48},{48,56},{56,32},{64,72... | collective-permute-start | bytes 921608 | tf_op jit(solution)/shard_map/ppermute | solution.py:35
  119.3 13.6 %collective-permute-start.17 = (bf16[160,960]{1,0:T(8,128)(2,1)}, bf16[160,960]{1,0:T(8,128)(2,1)}, u32[]{:S(2)}, u32[]{:S(2)}) collective-permute-start(bf16[160,960]{1,0:T(8,128)(2,1)} %constant_dynamic-update-slice_fusion.2.refs_0_), channel_id=1, source_target_pairs={{0,16},{8,24},{16,0},{24,8},{32,48},{40,56},{48,32},{56,40},{64,80... | collective-permute-start | bytes 921608 | tf_op jit(solution)/shard_map/ppermute | solution.py:35
  123.3 10.1 %collective-permute-start.18 = (bf16[160,960]{1,0:T(8,128)(2,1)}, bf16[160,960]{1,0:T(8,128)(2,1)}, u32[]{:S(2)}, u32[]{:S(2)}) collective-permute-start(bf16[160,960]{1,0:T(8,128)(2,1)} %constant_dynamic-update-slice_fusion.2.refs_0_), channel_id=1, source_target_pairs={{0,24},{8,0},{16,8},{24,16},{32,56},{40,32},{48,40},{56,48},{64,88... | collective-permute-start | bytes 921608 | tf_op jit(solution)/shard_map/ppermute | solution.py:35
  140.8 21.9 %collective-permute-start.22 = (bf16[160,2048]{1,0:T(8,128)(2,1)S(1)}, bf16[160,2048]{1,0:T(8,128)(2,1)S(1)}, u32[]{:S(2)}, u32[]{:S(2)}) collective-permute-start(bf16[160,2048]{1,0:T(8,128)(2,1)S(1)} %get-tuple-element.35), channel_id=1, source_target_pairs={{0,1},{1,0},{2,3},{3,2},{4,5},{5,4},{6,7},{7,6},{8,9},{9,8},{10,11... | collective-permute-start | bytes 1966088 | tf_op jit(solution)/shard_map/ppermute | solution.py:322
  163.8 14.7 %all-to-all-start = ((bf16[4,40,2048]{2,1,0:T(8,128)(2,1)}), bf16[4,40,2048]{2,1,0:T(8,128)(2,1)}, u32[]{:S(2)}, u32[]{:S(2)}) async-start(bf16[4,40,2048]{2,1,0:T(8,128)(2,1)} %bitcast.13), calls=%async_computation | async-start | bytes 1310720 | tf_op jit(solution)/shard_map/all_to_all | solution.py:328
  194.1 8.6 %collective-permute-start.23 = (bf16[160,2048]{1,0:T(8,128)(2,1)}, bf16[160,2048]{1,0:T(8,128)(2,1)}, u32[]{:S(2)}, u32[]{:S(2)}) collective-permute-start(bf16[160,2048]{1,0:T(8,128)(2,1)} %all_gather.10.mine_ref), channel_id=1, source_target_pairs={{0,1},{1,0},{2,3},{3,2},{4,5},{5,4},{6,7},{7,6},{8,9},{9,8},{10,11... | collective-permute-start | bytes 1966088 | tf_op jit(solution)/shard_map/ppermute | solution.py:322
  (72 other events, 1034.0 us)
where the time goes:
time: 268 us; the launch traced here: 266 us
  starting transfers between devices  118 us (44%)
  blocking collectives  59.3 us (22%)
  waiting for transfers between devices  39.1 us (15%)
  local copies, waits for them, and re-layouts  27.8 us (10%)
  Pallas kernels  18.4 us (7%)
    ppermute x22, starting transfers between devices, shift(): return lax.ppermute(array, 'fs', fs_shift(dy, dz))  76.3 us
    ppermute x5, starting transfers between devices, core_swap(): return lax.ppermute(array, 'tp', [(k, k ^ 1) for k in range(8)])  37.8 us
    all_to_all x2, blocking collectives, shares_of_rows(): lax.all_to_all(tiles, 'tp', 0, 0, tiled=True, axis_index_groups=X_GROUPS)  26 us
    unnamed x150, local copies, waits for them, and re-layouts  23.2 us
    all_gather x2, blocking collectives, rows_of_all(): lax.all_gather(normed, 'tp', axis=0, tiled=True, axis_index_groups=X_GROUPS)  22 us
    ppermute x22, waiting for transfers between devices, shift(): return lax.ppermute(array, 'fs', fs_shift(dy, dz))  21.8 us
    all_gather x1, blocking collectives, body(): lax.all_gather(first, 'fs', axis=0, tiled=True, axis_index_groups=groups)  11.2 us
    all_to_all x1, waiting for transfers between devices, shares_of_rows(): lax.all_to_all(tiles, 'tp', 0, 0, tiled=True, axis_index_groups=X_GROUPS)  8.71 us
  transfers between devices with their start and end apart: 28, of which 17 were waited for; matrix products, arithmetic and copies ran while one was open for 2% of the time, Pallas kernels for 1%

commit v1 on v0

--- a/solution.py
+++ b/solution.py
@@ -14,6 +14,9 @@
 F32 = jnp.float32
 VMEM = pl.BlockSpec(memory_space=pltpu.VMEM)
 SMEM = pl.BlockSpec(memory_space=pltpu.SMEM)
+
+
+LARGE = 63
 
 
 def limit(mib):
@@ -124,42 +127,44 @@
     return values * lax.rsqrt(jnp.mean(values * values, axis=-1, keepdims=True) + 1e-06) * gain
 
 
-def settle_kernel(factor, parts_ref, stream_ref, gain_ref, next_ref, new_ref, normed_ref):
+def settle_kernel(factor, row, parts_ref, stream_ref, gain_ref, new_ref, normed_ref):
     total = parts_ref[0].astype(F32)
     for k in range(1, parts_ref.shape[0]):
         total = total + parts_ref[k].astype(F32)
-    stream = stream_ref[...] + factor * rms_scale(total, gain_ref[...])
+    stream = stream_ref[...] + factor * rms_scale(total, gain_ref[row : row + 1, :])
     new_ref[...] = stream
-    normed_ref[...] = rms_scale(stream, next_ref[...]).astype(BF)
-
-
-def settle(parts, stream, gain, next_gain, factor):
-    return pl.pallas_call(
-        functools.partial(settle_kernel, factor),
+    normed = rms_scale(stream, gain_ref[row + 1 : row + 2, :]).astype(BF)
+    for k in range(normed_ref.shape[0]):
+        normed_ref[k] = normed
+
+
+def settle(parts, stream, gains, row, factor):
+    return pl.pallas_call(
+        functools.partial(settle_kernel, factor, row),
         out_shape=(
             jax.ShapeDtypeStruct(stream.shape, F32),
-            jax.ShapeDtypeStruct(stream.shape, BF),
+            jax.ShapeDtypeStruct((4, *stream.shape), BF),
         ),
-        in_specs=[VMEM] * 4,
+        in_specs=[VMEM] * 3,
         out_specs=(VMEM, VMEM),
         compiler_params=limit(6),
         cost_estimate=pl.CostEstimate(flops=10**8, bytes_accessed=1 << 20, transcendentals=0),
         name="settle",
-    )(parts, stream, gain, next_gain)
+    )(parts, stream, gains)
 
 
 def finish_kernel(at_ref, parts_ref, stream_ref, gain_ref, out_ref):
     total = parts_ref[0].astype(F32)
     for k in range(1, parts_ref.shape[0]):
         total = total + parts_ref[k].astype(F32)
-    result = (stream_ref[...] + 0.5 * rms_scale(total, gain_ref[...])).astype(BF)
+    result = (stream_ref[...] + 0.5 * rms_scale(total, gain_ref[5:6, :])).astype(BF)
     blocks = result.shape[1] // 128
     for p in range(blocks):
         start = pl.multiple_of(lax.rem(at_ref[0] + p, blocks) * 128, 128)
         out_ref[:, pl.ds(start, 128)] = result[:, p * 128 : (p + 1) * 128]
 
 
-def finish(at, parts, stream, gain):
+def finish(at, parts, stream, gains):
     return pl.pallas_call(
         finish_kernel,
         out_shape=jax.ShapeDtypeStruct(stream.shape, BF),
@@ -168,30 +173,42 @@
         compiler_params=limit(6),
         cost_estimate=pl.CostEstimate(flops=10**8, bytes_accessed=1 << 20, transcendentals=0),
         name="finish",
-    )(at, parts, stream, gain)
+    )(at, parts, stream, gains)
+
+
+def act(gate, up):
+    return (gate / (1.0 + jnp.exp(-gate)) * up).astype(BF)
 
 
 def gated_kernel(width, parts, *refs):
-    payloads, out_ref, w_ref = refs[parts : parts + NZ], refs[-2], refs[-1]
+    ins, out_ref = refs[: parts + NZ], refs[parts + NZ]
+    x_ref, w_ref, total_ref, sems = refs[parts + NZ + 1 :]
+    copies, at = [], 0
+    for k in range(parts):
+        rows = ins[k].shape[0]
+        copies.append(pltpu.make_async_copy(ins[k], x_ref.at[at : at + rows], sems.at[k]))
+        at += rows
     for k in range(NZ):
-        w_ref[k * 128 : (k + 1) * 128, :] = payloads[k][0:128, :]
-    x = jnp.concatenate([ref[...] for ref in refs[:parts]], axis=0)
+        rows = w_ref.at[k * 128 : (k + 1) * 128]
+        src = ins[parts + k].at[0:128]
+        copies.append(pltpu.make_async_copy(src, rows, sems.at[parts + k]))
+    for copy in copies:
+        copy.start()
+    for copy in copies[:parts]:
+        copy.wait()
+    step = 4
+    for k in range(0, NZ, step):
+        for copy in copies[parts + k : parts + k + step]:
+            copy.wait()
+        deep = slice(k * 128, (k + step) * 128)
+        for at in range(0, 2 * width, 256):
+            end = min(at + 256, 2 * width)
+            part = jnp.dot(x_ref[:, deep], w_ref[deep, at:end], preferred_element_type=F32)
+            total_ref[:, at:end] = part if k == 0 else total_ref[:, at:end] + part
     whole = width // 128 * 128
-
-    def act(gate, up):
-        return (gate / (1.0 + jnp.exp(-gate)) * up).astype(BF)
-
-    at = 0
-    while at < whole:
-        n = min(256, whole - at)
-        gate = jnp.dot(x, w_ref[:, at : at + n], preferred_element_type=F32)
-        up = jnp.dot(x, w_ref[:, whole + at : whole + at + n], preferred_element_type=F32)
-        out_ref[:, at : at + n] = act(gate, up)
-        at += n
-    if width > whole:
-        rest = width - whole
-        both = jnp.dot(x, w_ref[:, 2 * whole :], preferred_element_type=F32)
-        out_ref[:, whole:] = act(both[:, :rest], both[:, rest:])
+    out_ref[:, :whole] = act(total_ref[:, :whole], total_ref[:, whole : 2 * whole])
+    both = total_ref[:, 2 * whole :]
+    out_ref[:, whole:] = act(both[:, : width - whole], both[:, width - whole :])
 
 
 def gated(xs, payloads, width):
@@ -199,10 +216,15 @@
     return pl.pallas_call(
         functools.partial(gated_kernel, width, len(xs)),
         out_shape=jax.ShapeDtypeStruct((rows, width), BF),
-        in_specs=[VMEM] * (len(xs) + NZ),
+        in_specs=[HBM] * (len(xs) + NZ),
         out_specs=VMEM,
-        scratch_shapes=[pltpu.VMEM((depth, 2 * width), BF)],
-        compiler_params=limit(24),
+        scratch_shapes=[
+            pltpu.VMEM((rows, depth), BF),
+            pltpu.VMEM((depth, 2 * width), BF),
+            pltpu.VMEM((rows, 2 * width), F32),
+            pltpu.SemaphoreType.DMA((len(xs) + NZ,)),
+        ],
+        compiler_params=limit(LARGE),
         cost_estimate=pl.CostEstimate(
             flops=4 * rows * depth * width, bytes_accessed=8 << 20, transcendentals=0
         ),
@@ -210,62 +232,99 @@
     )(*xs, *payloads)
 
 
-def assemble_kernel(batch, y_ref, *refs):
-    ins, mix_ref, down_ref = refs[:NY], refs[-2], refs[-1]
-    y = y_ref[0]
-    width = mix_ref.shape[1] + down_ref.shape[1]
-    for j in range(NY):
-        owner = lax.rem(y - j + NY, NY)
-        for i, offset in enumerate(batch):
-            start = pl.multiple_of(OFFSETS.index(offset) * 128 + owner * 32, 32)
-            mix_ref[pl.ds(start, 32), :] = ins[j][i * 32 : (i + 1) * 32, 0:256]
-            down_ref[pl.ds(start, 32), :] = ins[j][i * 32 : (i + 1) * 32, 256:width]
-
-
-def assemble(y, pieces, batch, down_width, before=()):
-    rows = NZ * NY * 32
-    return pl.pallas_call(
-        functools.partial(assemble_kernel, batch),
-        out_shape=(
-            jax.ShapeDtypeStruct((rows, 256), BF),
-            jax.ShapeDtypeStruct((rows, down_width), BF),
-        ),
-        in_specs=[SMEM] + [VMEM] * (NY + len(before)),
-        out_specs=(VMEM, VMEM),
-        input_output_aliases={1 + NY: 0, 2 + NY: 1} if before else {},
-        compiler_params=limit(12),
-        cost_estimate=pl.CostEstimate(flops=10**8, bytes_accessed=8 << 20, transcendentals=0),
-        name="assemble",
-    )(y, *pieces, *before)
-
-
-def down_kernel(h_ref, w_ref, mine_ref, other_ref):
+def collect_kernel(*refs):
+    ins, out_ref, held_ref, sems = refs[:-3], refs[-3], refs[-2], refs[-1]
+    copies = []
+    for k, ref in enumerate(ins):
+        rows = held_ref.at[k * 32 : (k + 1) * 32]
+        if ref.shape[0] == 32:
+            copies.append(pltpu.make_async_copy(ref, rows, sems.at[k]))
+        else:
+            copies.append(pltpu.make_async_copy(ref.at[128:160], rows, sems.at[k]))
+        copies[-1].start()
+    for copy in copies:
+        copy.wait()
+    out_ref[...] = held_ref[:, 0 : out_ref.shape[1]]
+
+
+def collect(blocks, width):
+    rows = 32 * len(blocks)
+    return pl.pallas_call(
+        collect_kernel,
+        out_shape=jax.ShapeDtypeStruct((rows, width), BF),
+        in_specs=[HBM] * len(blocks),
+        out_specs=VMEM,
+        scratch_shapes=[
+            pltpu.VMEM((rows, blocks[0].shape[1]), BF),
+            pltpu.SemaphoreType.DMA((len(blocks),)),
+        ],
+        compiler_params=limit(LARGE),
+        cost_estimate=pl.CostEstimate(flops=10**8, bytes_accessed=1 << 20, transcendentals=0),
+        name="collect",
+    )(*blocks)
+
+
+def gather_copies(y, pieces, held_ref, sems, columns):
+    copies = {}
+    for b, batch in enumerate(BATCHES):
+        for j in range(NY):
+            owner = lax.rem(y - j + NY, NY)
+            for i, offset in enumerate(batch):
+                p = OFFSETS.index(offset)
+                start = pl.multiple_of(p * 128 + owner * 32, 32)
+                src = pieces[NY * b + j]
+                if columns is None:
+                    src = src.at[i * 32 : (i + 1) * 32]
+                else:
+                    src = src.at[i * 32 : (i + 1) * 32, 0:columns]
+                rows = held_ref.at[pl.ds(start, 32)]
+                copies[p, j] = pltpu.make_async_copy(src, rows, sems.at[p * NY + j])
+    for p in range(NZ):
+        for j in range(NY):
+            copies[p, j].start()
+    return copies
+
+
+def down_kernel(y_ref, h_ref, *refs):
+    pieces, mine_ref, other_ref, held_ref, sems = refs[:-4], refs[-4], refs[-3], refs[-2], refs[-1]
+    copies = gather_copies(y_ref[0], pieces, held_ref, sems, None)
     h = h_ref[...]
     half = h.shape[0] // 2
-    for at in range(0, w_ref.shape[0], 256):
+    for at in range(0, held_ref.shape[0], 256):
+        for p in range(at // 128, at // 128 + 2):
+            for j in range(NY):
+                copies[p, j].wait()
         share = lax.dot_general(
-            h, w_ref[at : at + 256, :], (((1,), (1,)), ((), ())), preferred_element_type=F32
+            h, held_ref[at : at + 256, 256:], (((1,), (1,)), ((), ())), preferred_element_type=F32
         ).astype(BF)
         mine_ref[:, at : at + 256] = share[:half]
         other_ref[:, at : at + 256] = share[half:]
 
 
-def down(hidden, w):
-    rows, out = hidden.shape[0], w.shape[0]
+def down(y, hidden, pieces):
+    rows, out = hidden.shape[0], NZ * NY * 32
     return pl.pallas_call(
         down_kernel,
         out_shape=(jax.ShapeDtypeStruct((rows // 2, out), BF),) * 2,
-        in_specs=[VMEM, VMEM],
+        in_specs=[SMEM, VMEM] + [HBM] * len(pieces),
         out_specs=(VMEM, VMEM),
-        compiler_params=limit(14),
+        scratch_shapes=[
+            pltpu.VMEM((out, pieces[0].shape[1]), BF),
+            pltpu.SemaphoreType.DMA((NZ * NY,)),
+        ],
+        compiler_params=limit(LARGE - 2),
         cost_estimate=pl.CostEstimate(
-            flops=2 * rows * out * w.shape[1], bytes_accessed=4 << 20, transcendentals=0
+            flops=2 * rows * out * hidden.shape[1], bytes_accessed=4 << 20, transcendentals=0
         ),
         name="down",
-    )(hidden, w)
-
-
-def mixer_kernel(kind_ref, mine_ref, other_ref, w_ref, pool_ref, scale_ref, keep_ref, send_ref):
+    )(y, hidden, *pieces)
+
+
+def mixer_kernel(kind_ref, mine_ref, other_ref, pool_ref, scale_ref, *refs):
+    pieces, keep_ref, send_ref, w_ref, sems = refs[:-4], refs[-4], refs[-3], refs[-2], refs[-1]
+    copies = gather_copies(kind_ref[2], pieces, w_ref, sems, 256)
+    for copy in copies.values():
+        copy.wait()
     rows = 2 * mine_ref.shape[0]
     tile = rows // 8
     kind, core = kind_ref[0], kind_ref[1]
@@ -300,19 +359,20 @@
         send_ref[:, at : at + 256] = share[rows // 2 :]
 
 
-def mixer(kind, mine, other, w, pool_w, pool_scale):
+def mixer(kind, mine, other, pool_w, pool_scale, pieces):
     rows, depth = 2 * mine.shape[0], mine.shape[1]
     return pl.pallas_call(
         mixer_kernel,
         out_shape=(jax.ShapeDtypeStruct((rows // 2, depth), BF),) * 2,
-        in_specs=[SMEM] + [VMEM] * 5,
+        in_specs=[SMEM] + [VMEM] * 4 + [HBM] * len(pieces),
         out_specs=(VMEM, VMEM),
-        compiler_params=limit(14),
+        scratch_shapes=[pltpu.VMEM((depth, 256), BF), pltpu.SemaphoreType.DMA((NZ * NY,))],
+        compiler_params=limit(LARGE - 4),
         cost_estimate=pl.CostEstimate(
             flops=4 * rows * depth * 128, bytes_accessed=4 << 20, transcendentals=0
         ),
         name="mixer",
-    )(kind, mine, other, w, pool_w, pool_scale)
+    )(kind, mine, other, pool_w, pool_scale, *pieces)
 
 
 X_GROUPS = [[2 * x + core for x in range(4)] for core in range(2)]
@@ -328,8 +388,9 @@
     return lax.all_to_all(tiles, "tp", 0, 0, tiled=True, axis_index_groups=X_GROUPS)
 
 
-def rows_of_all(normed):
-    mine = lax.all_gather(normed, "tp", axis=0, tiled=True, axis_index_groups=X_GROUPS)
+def rows_of_all(copies):
+    mine = lax.all_to_all(copies, "tp", 0, 0, tiled=True, axis_index_groups=X_GROUPS)
+    mine = mine.reshape(-1, copies.shape[-1])
     return mine, core_swap(mine)
 
 
@@ -348,43 +409,40 @@
     first_block = lax.rem(z + 8, NZ)
     core = lax.rem(tp_at, 2)
     gains = rolled(norm_gains, first_block)
-    gain = [gains[k : k + 1] for k in range(6)]
     numbers = jnp.stack([first_block, core, lax.rem(tp_at, 4), y]).astype(jnp.int32)
 
     back = ahead = jnp.concatenate([first, second], axis=0)
     got = {0: back}
     for k in range(1, 9):
         if k == 7:
-            last_second = shift(back[128:, :second_width], dz=2)
-        back = got[-k] = shift(back if k < 8 else back[:128], dz=1)
+            last_second = shift(back[128:], dz=2)
+        back = got[-k] = shift(back, dz=1)
         if k < 8:
             ahead = got[k] = shift(ahead, dz=-1)
         if k == 2:
             back, late_tokens = lax.optimization_barrier((back, tokens))
-            x = first_norm(numbers[0:2], late_tokens, gain[0])
+            x = first_norm(numbers[0:2], late_tokens, gains)
         if k == 5:
             back, x = lax.optimization_barrier((back, x))
         got[-k] = back
     payloads = [got[k] for k in OFFSETS]
 
-    late = ()
+    pieces = []
     for batch in BATCHES:
-        own = [last_second if s == -8 else got[s][128:, :second_width] for s in batch]
-        own = jnp.concatenate(own, axis=0)
-        pieces = [own, shift(own, dy=1), shift(own, dy=2), shift(own, dy=-1)]
-        late = assemble(numbers[3:4], pieces, batch, width, late)
-    mix_w, down_w = late
+        own = collect([last_second if s == -8 else got[s] for s in batch], second_width)
+        pieces += [own, shift(own, dy=1), shift(own, dy=2), shift(own, dy=-1)]
 
     stream = lax.dynamic_slice_in_dim(tokens, tp_at * own_rows, own_rows, 0)
     stream = rolled(stream, first_block).astype(F32)
-    parts = shares_of_rows(*down(gated([x], payloads, width), down_w))
-    stream, normed = settle(parts, stream, gain[1], gain[2], 0.5)
-    kind = jnp.stack([numbers[2], numbers[1]])
-    share = mixer(kind, *rows_of_all(normed), mix_w, pool_w[0], pool_scale[None])
-    stream, normed = settle(shares_of_rows(*share), stream, gain[3], gain[4], 1.0)
-    hidden = gated(rows_of_all(normed), payloads, width)
-    parts = shares_of_rows(*down(hidden, down_w))
-    return finish(numbers[0:1], parts, stream, gain[5])
+    hidden = gated([x], payloads, width)
+    parts = shares_of_rows(*down(numbers[3:4], hidden, pieces))
+    stream, copies = settle(parts, stream, gains, 1, 0.5)
+    kind = jnp.stack([numbers[2], numbers[1], numbers[3]])
+    share = mixer(kind, *rows_of_all(copies), pool_w[0], pool_scale[None], pieces)
+    stream, copies = settle(shares_of_rows(*share), stream, gains, 3, 1.0)
+    hidden = gated(rows_of_all(copies), payloads, width)
+    parts = shares_of_rows(*down(numbers[3:4], hidden, pieces))
+    return finish(numbers[0:1], parts, stream, gains)
 
 
 def solution(mesh):

time: 268 us -> 282 us (1.052)
  waiting for transfers between devices: 39.1 us -> 63.1 us
  local copies, waits for them, and re-layouts: 27.8 us -> 5.61 us
  Pallas kernels: 18.4 us -> 39.5 us
  starting transfers between devices: 118 us -> 105 us
  other arithmetic: 2.49 us -> 5.62 us
    all_to_all x0 -> x2, blocking collectives: none -> 23.8 us  [rows_of_all(): lax.all_to_all(copies, 'tp', 0, 0, tiled=True, axis_index_groups=X_GROUPS)]
    ppermute x22, waiting for transfers between devices: 21.8 us -> 45.4 us  [shift(): return lax.ppermute(array, 'fs', fs_shift(dy, dz))]
    all_gather x2 -> x0, blocking collectives: 22 us -> none  [rows_of_all(): lax.all_gather(normed, 'tp', axis=0, tiled=True, axis_index_groups=X_GROUPS)]
    unnamed x150 -> x29, local copies, waits for them, and re-layouts: 23.2 us -> 2.88 us
    pallas_call x2, Pallas kernels: 2.43 us -> 14.6 us  [down(): pl.pallas_call(down_kernel, out_shape=(jax.ShapeDtypeStruct((rows // 2, o...]
    ppermute x5, starting transfers between devices: 37.8 us -> 26.9 us  [core_swap(): return lax.ppermute(array, 'tp', [(k, k ^ 1) for k in range(8)])]
    pallas_call x2, Pallas kernels: 5.39 us -> 10.2 us  [gated(): pl.pallas_call(functools.partial(gated_kernel, width, len(xs)), out_shape...]
    convert_element_type x3, other arithmetic: 1.45 us -> 4.72 us  [shares_of_rows(): both = (mine.astype(F32) + core_swap(other).astype(F32)).astype(BF)]
  transfers between devices with their start and end apart: 28 -> 28, of which waited for: 17 -> 17; matrix products, arithmetic and copies ran while one was open for 2% -> 1% of each run, Pallas kernels for 1% -> 4%
where the time goes in v1:
time: 282 us; the launch traced here: 280 us
  starting transfers between devices  105 us (37%)
  waiting for transfers between devices  63.1 us (22%)
  blocking collectives  61 us (22%)
  Pallas kernels  39.5 us (14%)
  other arithmetic  5.62 us (2%)
  local copies, waits for them, and re-layouts  5.61 us (2%)
    ppermute x22, starting transfers between devices, shift(): return lax.ppermute(array, 'fs', fs_shift(dy, dz))  74 us
    ppermute x22, waiting for transfers between devices, shift(): return lax.ppermute(array, 'fs', fs_shift(dy, dz))  45.4 us
    ppermute x5, starting transfers between devices, core_swap(): return lax.ppermute(array, 'tp', [(k, k ^ 1) for k in range(8)])  26.9 us
    all_to_all x2, blocking collectives, shares_of_rows(): lax.all_to_all(tiles, 'tp', 0, 0, tiled=True, axis_index_groups=X_GROUPS)  26 us
    all_to_all x2, blocking collectives, rows_of_all(): lax.all_to_all(copies, 'tp', 0, 0, tiled=True, axis_index_groups=X_GROUPS)  23.8 us
    pallas_call x2, Pallas kernels, down(): pl.pallas_call(down_kernel, out_shape=(jax.ShapeDtypeStruct((rows // 2, o...  14.6 us
    all_gather x1, blocking collectives, body(): lax.all_gather(first, 'fs', axis=0, tiled=True, axis_index_groups=groups)  11.2 us
    pallas_call x2, Pallas kernels, gated(): pl.pallas_call(functools.partial(gated_kernel, width, len(xs)), out_shape...  10.2 us
  transfers between devices with their start and end apart: 28, of which 17 were waited for; matrix products, arithmetic and copies ran while one was open for 1% of the time, Pallas kernels for 4%

profile of v1, /device:TPU:1, one launch (start us, length us, event | category | flops | bytes accessed | tf_op | source)
XLA Modules:
  0.0 280.4 jit_solution(4674177722276204839)
XLA Ops:
  1.7 11.2 %all_gather.3 = bf16[128,1408]{1,0:T(8,128)(2,1)S(1)} all-gather(bf16[32,1408]{1,0:T(8,128)(2,1)} %get-tuple-element.21), channel_id=1, replica_groups={{0,8,16,24},{32,40,48,56},{64,72,80,88},{96,104,112,120},{128,136,144,1..., dimensions={0}, use_global_device_ids=true | all-gather | bytes 450560 | tf_op jit(solution)/shard_map/all_gather | solution.py:407
  18.4 9.5 %collective-permute-start.8 = (bf16[160,1408]{1,0:T(8,128)(2,1)S(1)}, bf16[160,1408]{1,0:T(8,128)(2,1)S(1)}, u32[]{:S(2)}, u32[]{:S(2)}) collective-permute-start(bf16[160,1408]{1,0:T(8,128)(2,1)S(1)} %constant_dynamic-update-slice_fusion.refs_9_.refs_0_.refs_10_), channel_id=1, source_target_pairs={{0,480},{8,488},{16,496},{24,504},{32,0},{40,8},{48,16},{56,24},{6... | collective-permute-start | bytes 1351688 | tf_op jit(solution)/shard_map/ppermute | solution.py:38
  27.9 6.2 %collective-permute-done.refs_8_.refs_1_.refs_9_ = bf16[160,1408]{1,0:T(8,128)(2,1)S(1)} collective-permute-done((bf16[160,1408]{1,0:T(8,128)(2,1)S(1)}, bf16[160,1408]{1,0:T(8,128)(2,1)S(1)}, u32[]{:S(2)}, u32[]{:S(2)}) %collective-permute-start) | collective-permute-done | bytes 450592 | tf_op jit(solution)/shard_map/ppermute | solution.py:38
  36.0 4.6 %collective-permute-start.9 = (bf16[160,1408]{1,0:T(8,128)(2,1)S(1)}, bf16[160,1408]{1,0:T(8,128)(2,1)S(1)}, u32[]{:S(2)}, u32[]{:S(2)}) collective-permute-start(bf16[160,1408]{1,0:T(8,128)(2,1)S(1)} %collective-permute-done.8.refs_10_.refs_2_.refs_11_), channel_id=1, source_target_pairs={{0,480},{8,488},{16,496},{24,504},{32,0},{40,8},{48,16},{56,24},{6... | collective-permute-start | bytes 1351688 | tf_op jit(solution)/shard_map/ppermute | solution.py:38
  40.6 5.3 %collective-permute-done.1.refs_7_.refs_3_.refs_8_ = bf16[160,1408]{1,0:T(8,128)(2,1)S(1)} collective-permute-done((bf16[160,1408]{1,0:T(8,128)(2,1)S(1)}, bf16[160,1408]{1,0:T(8,128)(2,1)S(1)}, u32[]{:S(2)}, u32[]{:S(2)}) %collective-permute-start.1) | collective-permute-done | bytes 450592 | tf_op jit(solution)/shard_map/ppermute | solution.py:38
  47.9 4.6 %collective-permute-start.10 = (bf16[160,1408]{1,0:T(8,128)(2,1)S(1)}, bf16[160,1408]{1,0:T(8,128)(2,1)}, u32[]{:S(2)}, u32[]{:S(2)}) collective-permute-start(bf16[160,1408]{1,0:T(8,128)(2,1)S(1)} %collective-permute-done.9.refs_11_.refs_4_.refs_12_), channel_id=1, source_target_pairs={{0,480},{8,488},{16,496},{24,504},{32,0},{40,8},{48,16},{56,24},{6... | collective-permute-start | bytes 1351688 | tf_op jit(solution)/shard_map/ppermute | solution.py:38
  58.9 4.6 %collective-permute-start.11 = (bf16[160,1408]{1,0:T(8,128)(2,1)}, bf16[160,1408]{1,0:T(8,128)(2,1)}, u32[]{:S(2)}, u32[]{:S(2)}) collective-permute-start(bf16[160,1408]{1,0:T(8,128)(2,1)} %collective-permute-done.10.refs_12_.refs_6_.refs_13_), channel_id=1, source_target_pairs={{0,480},{8,488},{16,496},{24,504},{32,0},{40,8},{48,16},{56,24},{6... | collective-permute-start | bytes 1351688 | tf_op jit(solution)/shard_map/ppermute | solution.py:38
  69.5 4.6 %collective-permute-start.12 = (bf16[160,1408]{1,0:T(8,128)(2,1)}, bf16[160,1408]{1,0:T(8,128)(2,1)}, u32[]{:S(2)}, u32[]{:S(2)}) collective-permute-start(bf16[160,1408]{1,0:T(8,128)(2,1)} %collective-permute-done.11.refs_13_.refs_8_.refs_14_), channel_id=1, source_target_pairs={{0,480},{8,488},{16,496},{24,504},{32,0},{40,8},{48,16},{56,24},{6... | collective-permute-start | bytes 1351688 | tf_op jit(solution)/shard_map/ppermute | solution.py:38
  80.0 4.8 %collective-permute-start.13 = (bf16[160,1408]{1,0:T(8,128)(2,1)}, bf16[160,1408]{1,0:T(8,128)(2,1)}, u32[]{:S(2)}, u32[]{:S(2)}) collective-permute-start(bf16[160,1408]{1,0:T(8,128)(2,1)} %collective-permute-done.12.refs_14_.refs_10_.refs_15_), channel_id=1, source_target_pairs={{0,480},{8,488},{16,496},{24,504},{32,0},{40,8},{48,16},{56,24},{6... | collective-permute-start | bytes 1351688 | tf_op jit(solution)/shard_map/ppermute | solution.py:38
  84.8 4.6 %collective-permute-done.5.refs_3_.refs_0_.refs_4_ = bf16[160,1408]{1,0:T(8,128)(2,1)} collective-permute-done((bf16[160,1408]{1,0:T(8,128)(2,1)}, bf16[160,1408]{1,0:T(8,128)(2,1)}, u32[]{:S(2)}, u32[]{:S(2)}) %collective-permute-start.5) | collective-permute-done | bytes 450592 | tf_op jit(solution)/shard_map/ppermute | solution.py:38
  97.2 4.6 %collective-permute-start.14 = (bf16[160,1408]{1,0:T(8,128)(2,1)}, bf16[160,1408]{1,0:T(8,128)(2,1)}, u32[]{:S(2)}, u32[]{:S(2)}) collective-permute-start(bf16[160,1408]{1,0:T(8,128)(2,1)} %collective-permute-done.13.refs_15_.refs_1_.refs_16_), channel_id=1, source_target_pairs={{0,480},{8,488},{16,496},{24,504},{32,0},{40,8},{48,16},{56,24},{6... | collective-permute-start | bytes 1351688 | tf_op jit(solution)/shard_map/ppermute | solution.py:38
  123.2 5.1 %gated.2.h_ref = bf16[320,704]{1,0:T(8,128)(2,1)} custom-call(bf16[320,2048]{1,0:T(8,128)(2,1)} %copy-done, bf16[160,1408]{1,0:T(8,128)(2,1)} %collective-permute-done.7.refs_1_.refs_2_, bf16[160,1408]{1,0:T(8,128)(2,1)} %collective-permute-done.6.refs_2_.refs_3_, bf16[160,1408]{1,0:T(8,128)(2,1)} %collective-permute-done.5.refs_3_.refs_0_.refs_4_, ...), custom_call_target="tpu_custom_call" | custom-call | flops 1845493760 | bytes 8388608 | tf_op jit(solution)/shard_map/gated/pallas_call | solution.py:216
  135.7 10.8 %collective-permute-done.19.refs_5_ = bf16[160,960]{1,0:T(8,128)(2,1)} collective-permute-done((bf16[160,960]{1,0:T(8,128)(2,1)}, bf16[160,960]{1,0:T(8,128)(2,1)}, u32[]{:S(2)}, u32[]{:S(2)}) %collective-permute-start.19) | collective-permute-done | bytes 307232 | tf_op jit(solution)/shard_map/ppermute | solution.py:38
  146.5 7.3 %down.2 = (bf16[160,2048]{1,0:T(8,128)(2,1)}, bf16[160,2048]{1,0:T(8,128)(2,1)}) custom-call(s32[1]{0:T(128)} %bitcast.1.y_ref, bf16[320,704]{1,0:T(8,128)(2,1)} %gated.2.h_ref, bf16[352,960]{1,0:T(8,128)(2,1)} %collect.2.refs_0_, bf16[352,960]{1,0:T(8,128)(2,1)} %collective-permute-done.15.refs_1_, bf16[352,960]{1,0:T(8,128)(2,1)} %collective-permute-done.16.refs_2_, ...), custom_call_target="tpu_custom_call" | custom-call | flops 922746880 | bytes 4194304 | tf_op jit(solution)/shard_map/down/pallas_call | solution.py:306
  153.8 13.7 %collective-permute-start.22 = (bf16[160,2048]{1,0:T(8,128)(2,1)}, bf16[160,2048]{1,0:T(8,128)(2,1)S(1)}, u32[]{:S(2)}, u32[]{:S(2)}) collective-permute-start(bf16[160,2048]{1,0:T(8,128)(2,1)} %get-tuple-element.28), channel_id=1, source_target_pairs={{0,1},{1,0},{2,3},{3,2},{4,5},{5,4},{6,7},{7,6},{8,9},{9,8},{10,11... | collective-permute-start | bytes 1966088 | tf_op jit(solution)/shard_map/ppermute | solution.py:382
  176.6 9.3 %all-to-all-done.parts_ref = bf16[4,40,2048]{2,1,0:T(8,128)(2,1)S(1)} async-done(((bf16[4,40,2048]{2,1,0:T(8,128)(2,1)}), bf16[4,40,2048]{2,1,0:T(8,128)(2,1)S(1)}, u32[]{:S(2)}, u32[]{:S(2)}) %all-to-all-start) | async-done | bytes 655392 | tf_op jit(solution)/shard_map/all_to_all | solution.py:388
  186.2 11.6 %all_to_all.25 = bf16[4,40,2048]{2,1,0:T(8,128)(2,1)S(1)} all-to-all(bf16[4,40,2048]{2,1,0:T(8,128)(2,1)S(1)} %get-tuple-element.29), channel_id=1, replica_groups={{0,2,4,6},{1,3,5,7},{8,10,12,14},{9,11,13,15},{16,18,20,22},{17,19,21,2..., dimensions={0} | all-to-all | bytes 1310720 | tf_op jit(solution)/shard_map/all_to_all | solution.py:392
  197.8 4.5 %collective-permute-start.23 = (bf16[160,2048]{1,0:T(8,128)(2,1)S(1)}, bf16[160,2048]{1,0:T(8,128)(2,1)S(1)}, u32[]{:S(2)}, u32[]{:S(2)}) collective-permute-start(bf16[160,2048]{1,0:T(8,128)(2,1)S(1)} %bitcast.15), channel_id=1, source_target_pairs={{0,1},{1,0},{2,3},{3,2},{4,5},{5,4},{6,7},{7,6},{8,9},{9,8},{10,11... | collective-permute-start | bytes 1966088 | tf_op jit(solution)/shard_map/ppermute | solution.py:382
  204.9 6.0 %mixer.1 = (bf16[160,2048]{1,0:T(8,128)(2,1)}, bf16[160,2048]{1,0:T(8,128)(2,1)}) custom-call(s32[3]{0:T(128)} %pad_add_fusion.kind_ref, bf16[160,2048]{1,0:T(8,128)(2,1)} %bitcast.16, bf16[160,2048]{1,0:T(8,128)(2,1)} %copy-done.11, bf16[128,128]{1,0:T(8,128)(2,1)} %bitcast.19, bf16[1,128]{1,0:T(2,128)(2,1)} %bitcast.20, bf16[352,960]{1,0:T(8,128)(2,1)} %collect.2.refs_0_, ...), custom_call_target="tpu_custom_call" | custom-call | flops 335544320 | bytes 4194304 | tf_op jit(solution)/shard_map/mixer/pallas_call | solution.py:364
  216.4 13.0 %all_to_all.26.parts_ref = bf16[4,40,2048]{2,1,0:T(8,128)(2,1)S(1)} all-to-all(bf16[4,40,2048]{2,1,0:T(8,128)(2,1)S(1)} %bitcast.17), channel_id=1, replica_groups={{0,2,4,6},{1,3,5,7},{8,10,12,14},{9,11,13,15},{16,18,20,22},{17,19,21,2..., dimensions={0} | all-to-all | bytes 1310720 | tf_op jit(solution)/shard_map/all_to_all | solution.py:388
  229.7 12.2 %all_to_all.27 = bf16[4,40,2048]{2,1,0:T(8,128)(2,1)S(1)} all-to-all(bf16[4,40,2048]{2,1,0:T(8,128)(2,1)S(1)} %get-tuple-element.33), channel_id=1, replica_groups={{0,2,4,6},{1,3,5,7},{8,10,12,14},{9,11,13,15},{16,18,20,22},{17,19,21,2..., dimensions={0} | all-to-all | bytes 1310720 | tf_op jit(solution)/shard_map/all_to_all | solution.py:392
  248.5 5.1 %gated.3.h_ref = bf16[320,704]{1,0:T(8,128)(2,1)} custom-call(bf16[160,2048]{1,0:T(8,128)(2,1)} %bitcast.14, bf16[160,2048]{1,0:T(8,128)(2,1)} %collective-permute-done.25.refs_1_, bf16[160,1408]{1,0:T(8,128)(2,1)} %collective-permute-done.7.refs_1_.refs_2_, bf16[160,1408]{1,0:T(8,128)(2,1)} %collective-permute-done.6.refs_2_.refs_3_, ...), custom_call_target="tpu_custom_call" | custom-call | flops 1845493760 | bytes 8388608 | tf_op jit(solution)/shard_map/gated/pallas_call | solution.py:216
  253.6 7.3 %down.3 = (bf16[160,2048]{1,0:T(8,128)(2,1)}, bf16[160,2048]{1,0:T(8,128)(2,1)}) custom-call(s32[1]{0:T(128)} %bitcast.1.y_ref, bf16[320,704]{1,0:T(8,128)(2,1)} %gated.3.h_ref, bf16[352,960]{1,0:T(8,128)(2,1)} %collect.2.refs_0_, bf16[352,960]{1,0:T(8,128)(2,1)} %collective-permute-done.15.refs_1_, bf16[352,960]{1,0:T(8,128)(2,1)} %collective-permute-done.16.refs_2_, ...), custom_call_target="tpu_custom_call" | custom-call | flops 922746880 | bytes 4194304 | tf_op jit(solution)/shard_map/down/pallas_call | solution.py:306
  266.5 13.0 %all_to_all.28.parts_ref = bf16[4,40,2048]{2,1,0:T(8,128)(2,1)S(1)} all-to-all(bf16[4,40,2048]{2,1,0:T(8,128)(2,1)S(1)} %bitcast.18), channel_id=1, replica_groups={{0,2,4,6},{1,3,5,7},{8,10,12,14},{9,11,13,15},{16,18,20,22},{17,19,21,2..., dimensions={0} | all-to-all | bytes 1310720 | tf_op jit(solution)/shard_map/all_to_all | solution.py:388
  (88 shorter events, 96.4 us)
Async XLA Ops:
  13.9 20.2 %collective-permute-start = (bf16[160,1408]{1,0:T(8,128)(2,1)S(1)}, bf16[160,1408]{1,0:T(8,128)(2,1)S(1)}, u32[]{:S(2)}, u32[]{:S(2)}) collective-permute-start(bf16[160,1408]{1,0:T(8,128)(2,1)S(1)} %constant_dynamic-update-slice_fusion.refs_9_.refs_0_.refs_10_), channel_id=1, source_target_pairs={{0,32},{8,40},{16,48},{24,56},{32,64},{40,72},{48,80},{56,88},{64,... | collective-permute-start | bytes 1351688 | tf_op jit(solution)/shard_map/ppermute | solution.py:38
  18.4 17.6 %collective-permute-start.8 = (bf16[160,1408]{1,0:T(8,128)(2,1)S(1)}, bf16[160,1408]{1,0:T(8,128)(2,1)S(1)}, u32[]{:S(2)}, u32[]{:S(2)}) collective-permute-start(bf16[160,1408]{1,0:T(8,128)(2,1)S(1)} %constant_dynamic-update-slice_fusion.refs_9_.refs_0_.refs_10_), channel_id=1, source_target_pairs={{0,480},{8,488},{16,496},{24,504},{32,0},{40,8},{48,16},{56,24},{6... | collective-permute-start | bytes 1351688 | tf_op jit(solution)/shard_map/ppermute | solution.py:38
  34.1 11.8 %collective-permute-start.1 = (bf16[160,1408]{1,0:T(8,128)(2,1)S(1)}, bf16[160,1408]{1,0:T(8,128)(2,1)S(1)}, u32[]{:S(2)}, u32[]{:S(2)}) collective-permute-start(bf16[160,1408]{1,0:T(8,128)(2,1)S(1)} %collective-permute-done.refs_8_.refs_1_.refs_9_), channel_id=1, source_target_pairs={{0,32},{8,40},{16,48},{24,56},{32,64},{40,72},{48,80},{56,88},{64,... | collective-permute-start | bytes 1351688 | tf_op jit(solution)/shard_map/ppermute | solution.py:38
  36.0 11.8 %collective-permute-start.9 = (bf16[160,1408]{1,0:T(8,128)(2,1)S(1)}, bf16[160,1408]{1,0:T(8,128)(2,1)S(1)}, u32[]{:S(2)}, u32[]{:S(2)}) collective-permute-start(bf16[160,1408]{1,0:T(8,128)(2,1)S(1)} %collective-permute-done.8.refs_10_.refs_2_.refs_11_), channel_id=1, source_target_pairs={{0,480},{8,488},{16,496},{24,504},{32,0},{40,8},{48,16},{56,24},{6... | collective-permute-start | bytes 1351688 | tf_op jit(solution)/shard_map/ppermute | solution.py:38
  46.0 11.0 %collective-permute-start.2 = (bf16[160,1408]{1,0:T(8,128)(2,1)S(1)}, bf16[160,1408]{1,0:T(8,128)(2,1)S(1)}, u32[]{:S(2)}, u32[]{:S(2)}) collective-permute-start(bf16[160,1408]{1,0:T(8,128)(2,1)S(1)} %collective-permute-done.1.refs_7_.refs_3_.refs_8_), channel_id=1, source_target_pairs={{0,32},{8,40},{16,48},{24,56},{32,64},{40,72},{48,80},{56,88},{64,... | collective-permute-start | bytes 1351688 | tf_op jit(solution)/shard_map/ppermute | solution.py:38
  47.9 11.0 %collective-permute-start.10 = (bf16[160,1408]{1,0:T(8,128)(2,1)S(1)}, bf16[160,1408]{1,0:T(8,128)(2,1)}, u32[]{:S(2)}, u32[]{:S(2)}) collective-permute-start(bf16[160,1408]{1,0:T(8,128)(2,1)S(1)} %collective-permute-done.9.refs_11_.refs_4_.refs_12_), channel_id=1, source_target_pairs={{0,480},{8,488},{16,496},{24,504},{32,0},{40,8},{48,16},{56,24},{6... | collective-permute-start | bytes 1351688 | tf_op jit(solution)/shard_map/ppermute | solution.py:38
  56.9 10.4 %collective-permute-start.3 = (bf16[160,1408]{1,0:T(8,128)(2,1)S(1)}, bf16[160,1408]{1,0:T(8,128)(2,1)}, u32[]{:S(2)}, u32[]{:S(2)}) collective-permute-start(bf16[160,1408]{1,0:T(8,128)(2,1)S(1)} %collective-permute-done.2.refs_6_.refs_5_.refs_7_), channel_id=1, source_target_pairs={{0,32},{8,40},{16,48},{24,56},{32,64},{40,72},{48,80},{56,88},{64,... | collective-permute-start | bytes 1351688 | tf_op jit(solution)/shard_map/ppermute | solution.py:38
  58.9 10.6 %collective-permute-start.11 = (bf16[160,1408]{1,0:T(8,128)(2,1)}, bf16[160,1408]{1,0:T(8,128)(2,1)}, u32[]{:S(2)}, u32[]{:S(2)}) collective-permute-start(bf16[160,1408]{1,0:T(8,128)(2,1)} %collective-permute-done.10.refs_12_.refs_6_.refs_13_), channel_id=1, source_target_pairs={{0,480},{8,488},{16,496},{24,504},{32,0},{40,8},{48,16},{56,24},{6... | collective-permute-start | bytes 1351688 | tf_op jit(solution)/shard_map/ppermute | solution.py:38
  67.4 10.7 %collective-permute-start.4 = (bf16[160,1408]{1,0:T(8,128)(2,1)}, bf16[160,1408]{1,0:T(8,128)(2,1)}, u32[]{:S(2)}, u32[]{:S(2)}) collective-permute-start(bf16[160,1408]{1,0:T(8,128)(2,1)} %collective-permute-done.3.refs_5_.refs_7_.refs_6_), channel_id=1, source_target_pairs={{0,32},{8,40},{16,48},{24,56},{32,64},{40,72},{48,80},{56,88},{64,... | collective-permute-start | bytes 1351688 | tf_op jit(solution)/shard_map/ppermute | solution.py:38
  69.5 10.5 %collective-permute-start.12 = (bf16[160,1408]{1,0:T(8,128)(2,1)}, bf16[160,1408]{1,0:T(8,128)(2,1)}, u32[]{:S(2)}, u32[]{:S(2)}) collective-permute-start(bf16[160,1408]{1,0:T(8,128)(2,1)} %collective-permute-done.11.refs_13_.refs_8_.refs_14_), channel_id=1, source_target_pairs={{0,480},{8,488},{16,496},{24,504},{32,0},{40,8},{48,16},{56,24},{6... | collective-permute-start | bytes 1351688 | tf_op jit(solution)/shard_map/ppermute | solution.py:38
  78.0 11.3 %collective-permute-start.5 = (bf16[160,1408]{1,0:T(8,128)(2,1)}, bf16[160,1408]{1,0:T(8,128)(2,1)}, u32[]{:S(2)}, u32[]{:S(2)}) collective-permute-start(bf16[160,1408]{1,0:T(8,128)(2,1)} %collective-permute-done.4.refs_4_.refs_9_.refs_5_), channel_id=1, source_target_pairs={{0,32},{8,40},{16,48},{24,56},{32,64},{40,72},{48,80},{56,88},{64,... | collective-permute-start | bytes 1351688 | tf_op jit(solution)/shard_map/ppermute | solution.py:38
  80.0 17.2 %collective-permute-start.13 = (bf16[160,1408]{1,0:T(8,128)(2,1)}, bf16[160,1408]{1,0:T(8,128)(2,1)}, u32[]{:S(2)}, u32[]{:S(2)}) collective-permute-start(bf16[160,1408]{1,0:T(8,128)(2,1)} %collective-permute-done.12.refs_14_.refs_10_.refs_15_), channel_id=1, source_target_pairs={{0,480},{8,488},{16,496},{24,504},{32,0},{40,8},{48,16},{56,24},{6... | collective-permute-start | bytes 1351688 | tf_op jit(solution)/shard_map/ppermute | solution.py:38
  89.3 15.2 %collective-permute-start.6 = (bf16[160,1408]{1,0:T(8,128)(2,1)}, bf16[160,1408]{1,0:T(8,128)(2,1)}, u32[]{:S(2)}, u32[]{:S(2)}) collective-permute-start(bf16[160,1408]{1,0:T(8,128)(2,1)} %collective-permute-done.5.refs_3_.refs_0_.refs_4_), channel_id=1, source_target_pairs={{0,32},{8,40},{16,48},{24,56},{32,64},{40,72},{48,80},{56,88},{64,... | collective-permute-start | bytes 1351688 | tf_op jit(solution)/shard_map/ppermute | solution.py:38
  93.6 25.1 %collective-permute-start.17 = (bf16[352,960]{1,0:T(8,128)(2,1)}, bf16[352,960]{1,0:T(8,128)(2,1)S(1)}, u32[]{:S(2)}, u32[]{:S(2)}) collective-permute-start(bf16[352,960]{1,0:T(8,128)(2,1)} %collect.2.refs_0_), channel_id=1, source_target_pairs={{0,24},{8,0},{16,8},{24,16},{32,56},{40,32},{48,40},{56,48},{64,88... | collective-permute-start | bytes 2027528 | tf_op jit(solution)/shard_map/ppermute | solution.py:38
  97.2 15.5 %collective-permute-start.14 = (bf16[160,1408]{1,0:T(8,128)(2,1)}, bf16[160,1408]{1,0:T(8,128)(2,1)}, u32[]{:S(2)}, u32[]{:S(2)}) collective-permute-start(bf16[160,1408]{1,0:T(8,128)(2,1)} %collective-permute-done.13.refs_15_.refs_1_.refs_16_), channel_id=1, source_target_pairs={{0,480},{8,488},{16,496},{24,504},{32,0},{40,8},{48,16},{56,24},{6... | collective-permute-start | bytes 1351688 | tf_op jit(solution)/shard_map/ppermute | solution.py:38
  102.6 7.7 %collective-permute-start.18 = (bf16[32,1408]{1,0:T(8,128)(2,1)S(1)}, bf16[32,1408]{1,0:T(8,128)(2,1)S(1)}, u32[]{:S(2)}, u32[]{:S(2)}) collective-permute-start(bf16[32,1408]{1,0:T(8,128)(2,1)S(1)} %slice.4), channel_id=1, source_target_pairs={{0,64},{8,72},{16,80},{24,88},{32,96},{40,104},{48,112},{56,120},{... | collective-permute-start | bytes 270344 | tf_op jit(solution)/shard_map/ppermute | solution.py:38
  104.6 16.1 %collective-permute-start.7 = (bf16[160,1408]{1,0:T(8,128)(2,1)}, bf16[160,1408]{1,0:T(8,128)(2,1)}, u32[]{:S(2)}, u32[]{:S(2)}) collective-permute-start(bf16[160,1408]{1,0:T(8,128)(2,1)} %collective-permute-done.6.refs_2_.refs_3_), channel_id=1, source_target_pairs={{0,32},{8,40},{16,48},{24,56},{32,64},{40,72},{48,80},{56,88},{64,... | collective-permute-start | bytes 1351688 | tf_op jit(solution)/shard_map/ppermute | solution.py:38
  106.5 21.8 %collective-permute-start.16 = (bf16[352,960]{1,0:T(8,128)(2,1)}, bf16[352,960]{1,0:T(8,128)(2,1)}, u32[]{:S(2)}, u32[]{:S(2)}) collective-permute-start(bf16[352,960]{1,0:T(8,128)(2,1)} %collect.2.refs_0_), channel_id=1, source_target_pairs={{0,16},{8,24},{16,0},{24,8},{32,48},{40,56},{48,32},{56,40},{64,80... | collective-permute-start | bytes 2027528 | tf_op jit(solution)/shard_map/ppermute | solution.py:38
  110.3 18.2 %collective-permute-start.15 = (bf16[352,960]{1,0:T(8,128)(2,1)}, bf16[352,960]{1,0:T(8,128)(2,1)}, u32[]{:S(2)}, u32[]{:S(2)}) collective-permute-start(bf16[352,960]{1,0:T(8,128)(2,1)} %collect.2.refs_0_), channel_id=1, source_target_pairs={{0,8},{8,16},{16,24},{24,0},{32,40},{40,48},{48,56},{56,32},{64,72... | collective-permute-start | bytes 2027528 | tf_op jit(solution)/shard_map/ppermute | solution.py:38
  114.6 18.1 %collective-permute-start.21 = (bf16[160,960]{1,0:T(8,128)(2,1)}, bf16[160,960]{1,0:T(8,128)(2,1)}, u32[]{:S(2)}, u32[]{:S(2)}) collective-permute-start(bf16[160,960]{1,0:T(8,128)(2,1)} %collect.3.refs_4_), channel_id=1, source_target_pairs={{0,24},{8,0},{16,8},{24,16},{32,56},{40,32},{48,40},{56,48},{64,88... | collective-permute-start | bytes 921608 | tf_op jit(solution)/shard_map/ppermute | solution.py:38
  118.7 17.0 %collective-permute-start.20 = (bf16[160,960]{1,0:T(8,128)(2,1)}, bf16[160,960]{1,0:T(8,128)(2,1)}, u32[]{:S(2)}, u32[]{:S(2)}) collective-permute-start(bf16[160,960]{1,0:T(8,128)(2,1)} %collect.3.refs_4_), channel_id=1, source_target_pairs={{0,16},{8,24},{16,0},{24,8},{32,48},{40,56},{48,32},{56,40},{64,80... | collective-permute-start | bytes 921608 | tf_op jit(solution)/shard_map/ppermute | solution.py:38
  120.7 25.8 %collective-permute-start.19 = (bf16[160,960]{1,0:T(8,128)(2,1)}, bf16[160,960]{1,0:T(8,128)(2,1)}, u32[]{:S(2)}, u32[]{:S(2)}) collective-permute-start(bf16[160,960]{1,0:T(8,128)(2,1)} %collect.3.refs_4_), channel_id=1, source_target_pairs={{0,8},{8,16},{16,24},{24,0},{32,40},{40,48},{48,56},{56,32},{64,72... | collective-permute-start | bytes 921608 | tf_op jit(solution)/shard_map/ppermute | solution.py:38
  153.8 15.6 %collective-permute-start.22 = (bf16[160,2048]{1,0:T(8,128)(2,1)}, bf16[160,2048]{1,0:T(8,128)(2,1)S(1)}, u32[]{:S(2)}, u32[]{:S(2)}) collective-permute-start(bf16[160,2048]{1,0:T(8,128)(2,1)} %get-tuple-element.28), channel_id=1, source_target_pairs={{0,1},{1,0},{2,3},{3,2},{4,5},{5,4},{6,7},{7,6},{8,9},{9,8},{10,11... | collective-permute-start | bytes 1966088 | tf_op jit(solution)/shard_map/ppermute | solution.py:382
  171.6 14.3 %all-to-all-start = ((bf16[4,40,2048]{2,1,0:T(8,128)(2,1)}), bf16[4,40,2048]{2,1,0:T(8,128)(2,1)S(1)}, u32[]{:S(2)}, u32[]{:S(2)}) async-start(bf16[4,40,2048]{2,1,0:T(8,128)(2,1)} %bitcast.6), calls=%async_computation | async-start | bytes 1310720 | tf_op jit(solution)/shard_map/all_to_all | solution.py:388
  (18 other events, 365.1 us)

commit v2 on v0

--- a/solution.py
+++ b/solution.py
@@ -124,42 +124,44 @@
     return values * lax.rsqrt(jnp.mean(values * values, axis=-1, keepdims=True) + 1e-06) * gain
 
 
-def settle_kernel(factor, parts_ref, stream_ref, gain_ref, next_ref, new_ref, normed_ref):
+def settle_kernel(factor, row, parts_ref, stream_ref, gain_ref, new_ref, normed_ref):
     total = parts_ref[0].astype(F32)
     for k in range(1, parts_ref.shape[0]):
         total = total + parts_ref[k].astype(F32)
-    stream = stream_ref[...] + factor * rms_scale(total, gain_ref[...])
+    stream = stream_ref[...] + factor * rms_scale(total, gain_ref[row : row + 1, :])
     new_ref[...] = stream
-    normed_ref[...] = rms_scale(stream, next_ref[...]).astype(BF)
-
-
-def settle(parts, stream, gain, next_gain, factor):
-    return pl.pallas_call(
-        functools.partial(settle_kernel, factor),
+    normed = rms_scale(stream, gain_ref[row + 1 : row + 2, :]).astype(BF)
+    for k in range(normed_ref.shape[0]):
+        normed_ref[k] = normed
+
+
+def settle(parts, stream, gains, row, factor):
+    return pl.pallas_call(
+        functools.partial(settle_kernel, factor, row),
         out_shape=(
             jax.ShapeDtypeStruct(stream.shape, F32),
-            jax.ShapeDtypeStruct(stream.shape, BF),
-        ),
-        in_specs=[VMEM] * 4,
+            jax.ShapeDtypeStruct((4, *stream.shape), BF),
+        ),
+        in_specs=[VMEM] * 3,
         out_specs=(VMEM, VMEM),
         compiler_params=limit(6),
         cost_estimate=pl.CostEstimate(flops=10**8, bytes_accessed=1 << 20, transcendentals=0),
         name="settle",
-    )(parts, stream, gain, next_gain)
+    )(parts, stream, gains)
 
 
 def finish_kernel(at_ref, parts_ref, stream_ref, gain_ref, out_ref):
     total = parts_ref[0].astype(F32)
     for k in range(1, parts_ref.shape[0]):
         total = total + parts_ref[k].astype(F32)
-    result = (stream_ref[...] + 0.5 * rms_scale(total, gain_ref[...])).astype(BF)
+    result = (stream_ref[...] + 0.5 * rms_scale(total, gain_ref[5:6, :])).astype(BF)
     blocks = result.shape[1] // 128
     for p in range(blocks):
         start = pl.multiple_of(lax.rem(at_ref[0] + p, blocks) * 128, 128)
         out_ref[:, pl.ds(start, 128)] = result[:, p * 128 : (p + 1) * 128]
 
 
-def finish(at, parts, stream, gain):
+def finish(at, parts, stream, gains):
     return pl.pallas_call(
         finish_kernel,
         out_shape=jax.ShapeDtypeStruct(stream.shape, BF),
@@ -168,7 +170,11 @@
         compiler_params=limit(6),
         cost_estimate=pl.CostEstimate(flops=10**8, bytes_accessed=1 << 20, transcendentals=0),
         name="finish",
-    )(at, parts, stream, gain)
+    )(at, parts, stream, gains)
+
+
+def act(gate, up):
+    return (gate / (1.0 + jnp.exp(-gate)) * up).astype(BF)
 
 
 def gated_kernel(width, parts, *refs):
@@ -177,10 +183,6 @@
         w_ref[k * 128 : (k + 1) * 128, :] = payloads[k][0:128, :]
     x = jnp.concatenate([ref[...] for ref in refs[:parts]], axis=0)
     whole = width // 128 * 128
-
-    def act(gate, up):
-        return (gate / (1.0 + jnp.exp(-gate)) * up).astype(BF)
-
     at = 0
     while at < whole:
         n = min(256, whole - at)
@@ -188,10 +190,8 @@
         up = jnp.dot(x, w_ref[:, whole + at : whole + at + n], preferred_element_type=F32)
         out_ref[:, at : at + n] = act(gate, up)
         at += n
-    if width > whole:
-        rest = width - whole
-        both = jnp.dot(x, w_ref[:, 2 * whole :], preferred_element_type=F32)
-        out_ref[:, whole:] = act(both[:, :rest], both[:, rest:])
+    both = jnp.dot(x, w_ref[:, 2 * whole :], preferred_element_type=F32)
+    out_ref[:, whole:] = act(both[:, : width - whole], both[:, width - whole :])
 
 
 def gated(xs, payloads, width):
@@ -202,7 +202,7 @@
         in_specs=[VMEM] * (len(xs) + NZ),
         out_specs=VMEM,
         scratch_shapes=[pltpu.VMEM((depth, 2 * width), BF)],
-        compiler_params=limit(24),
+        compiler_params=limit(16),
         cost_estimate=pl.CostEstimate(
             flops=4 * rows * depth * width, bytes_accessed=8 << 20, transcendentals=0
         ),
@@ -210,33 +210,86 @@
     )(*xs, *payloads)
 
 
-def assemble_kernel(batch, y_ref, *refs):
-    ins, mix_ref, down_ref = refs[:NY], refs[-2], refs[-1]
+def absorb_kernel(places, x_ref, *refs):
+    n = len(places)
+    blocks, total_ref = refs[:n], refs[-1]
+    x = [x_ref[:, place * 128 : (place + 1) * 128] for place in places]
+    x = x[0] if n == 1 else jnp.concatenate(x, axis=1)
+    width = total_ref.shape[1]
+    for at in range(0, width, 256):
+        end = min(width, at + 256)
+        w = [block[0:128, at:end] for block in blocks]
+        w = w[0] if n == 1 else jnp.concatenate(w, axis=0)
+        part = jnp.dot(x, w, preferred_element_type=F32)
+        total_ref[:, at:end] = part if len(refs) == n + 1 else refs[n][:, at:end] + part
+
+
+def absorb(x, blocks, places, total=None):
+    rows, width, n = x.shape[0], blocks[0].shape[1], len(blocks)
+    carried = () if total is None else (total,)
+    return pl.pallas_call(
+        functools.partial(absorb_kernel, places),
+        out_shape=jax.ShapeDtypeStruct((rows, width), F32),
+        in_specs=[VMEM] * (1 + n + len(carried)),
+        out_specs=VMEM,
+        input_output_aliases={} if total is None else {1 + n: 0},
+        compiler_params=limit(6),
+        cost_estimate=pl.CostEstimate(
+            flops=2 * rows * width * 128 * n, bytes_accessed=n << 19, transcendentals=0
+        ),
+        name="absorb",
+    )(x, *blocks, *carried)
+
+
+def silu_kernel(total_ref, out_ref):
+    width = out_ref.shape[1]
+    whole = width // 128 * 128
+    out_ref[:, :whole] = act(total_ref[:, :whole], total_ref[:, whole : 2 * whole])
+    both = total_ref[:, 2 * whole :]
+    out_ref[:, whole:] = act(both[:, : width - whole], both[:, width - whole :])
+
+
+def silu(total):
+    rows, width = total.shape
+    return pl.pallas_call(
+        silu_kernel,
+        out_shape=jax.ShapeDtypeStruct((rows, width // 2), BF),
+        in_specs=[VMEM],
+        out_specs=VMEM,
+        compiler_params=limit(4),
+        cost_estimate=pl.CostEstimate(flops=10**8, bytes_accessed=1 << 20, transcendentals=0),
+        name="silu",
+    )(total)
+
+
+def assemble_kernel(y_ref, *refs):
+    ins, mix_ref, down_ref = refs[:-2], refs[-2], refs[-1]
     y = y_ref[0]
     width = mix_ref.shape[1] + down_ref.shape[1]
-    for j in range(NY):
-        owner = lax.rem(y - j + NY, NY)
-        for i, offset in enumerate(batch):
-            start = pl.multiple_of(OFFSETS.index(offset) * 128 + owner * 32, 32)
-            mix_ref[pl.ds(start, 32), :] = ins[j][i * 32 : (i + 1) * 32, 0:256]
-            down_ref[pl.ds(start, 32), :] = ins[j][i * 32 : (i + 1) * 32, 256:width]
-
-
-def assemble(y, pieces, batch, down_width, before=()):
+    for k, batch in enumerate(BATCHES):
+        for j in range(NY):
+            owner = lax.rem(y - j + NY, NY)
+            src = ins[NY * k + j]
+            for i, offset in enumerate(batch):
+                start = pl.multiple_of(OFFSETS.index(offset) * 128 + owner * 32, 32)
+                mix_ref[pl.ds(start, 32), :] = src[i * 32 : (i + 1) * 32, 0:256]
+                down_ref[pl.ds(start, 32), :] = src[i * 32 : (i + 1) * 32, 256:width]
+
+
+def assemble(y, pieces, down_width):
     rows = NZ * NY * 32
     return pl.pallas_call(
-        functools.partial(assemble_kernel, batch),
+        assemble_kernel,
         out_shape=(
             jax.ShapeDtypeStruct((rows, 256), BF),
             jax.ShapeDtypeStruct((rows, down_width), BF),
         ),
-        in_specs=[SMEM] + [VMEM] * (NY + len(before)),
+        in_specs=[SMEM] + [VMEM] * len(pieces),
         out_specs=(VMEM, VMEM),
-        input_output_aliases={1 + NY: 0, 2 + NY: 1} if before else {},
-        compiler_params=limit(12),
+        compiler_params=limit(14),
         cost_estimate=pl.CostEstimate(flops=10**8, bytes_accessed=8 << 20, transcendentals=0),
         name="assemble",
-    )(y, *pieces, *before)
+    )(y, *pieces)
 
 
 def down_kernel(h_ref, w_ref, mine_ref, other_ref):
@@ -328,8 +381,9 @@
     return lax.all_to_all(tiles, "tp", 0, 0, tiled=True, axis_index_groups=X_GROUPS)
 
 
-def rows_of_all(normed):
-    mine = lax.all_gather(normed, "tp", axis=0, tiled=True, axis_index_groups=X_GROUPS)
+def rows_of_all(copies):
+    mine = lax.all_to_all(copies, "tp", 0, 0, tiled=True, axis_index_groups=X_GROUPS)
+    mine = mine.reshape(-1, copies.shape[-1])
     return mine, core_swap(mine)
 
 
@@ -348,43 +402,41 @@
     first_block = lax.rem(z + 8, NZ)
     core = lax.rem(tp_at, 2)
     gains = rolled(norm_gains, first_block)
-    gain = [gains[k : k + 1] for k in range(6)]
     numbers = jnp.stack([first_block, core, lax.rem(tp_at, 4), y]).astype(jnp.int32)
 
+    first, late_tokens = lax.optimization_barrier((first, tokens))
     back = ahead = jnp.concatenate([first, second], axis=0)
+    x = first_norm(numbers[0:2], late_tokens, gains)
     got = {0: back}
+    total = None
     for k in range(1, 9):
         if k == 7:
             last_second = shift(back[128:, :second_width], dz=2)
-        back = got[-k] = shift(back if k < 8 else back[:128], dz=1)
+        back = got[-k] = shift(back, dz=1)
         if k < 8:
             ahead = got[k] = shift(ahead, dz=-1)
-        if k == 2:
-            back, late_tokens = lax.optimization_barrier((back, tokens))
-            x = first_norm(numbers[0:2], late_tokens, gain[0])
-        if k == 5:
-            back, x = lax.optimization_barrier((back, x))
-        got[-k] = back
+        places = ([0] if k == 1 else []) + [-k] + ([k] if k < 8 else [])
+        total = absorb(x, [got[p] for p in places], tuple(8 + p for p in places), total)
     payloads = [got[k] for k in OFFSETS]
 
-    late = ()
+    pieces = []
     for batch in BATCHES:
         own = [last_second if s == -8 else got[s][128:, :second_width] for s in batch]
         own = jnp.concatenate(own, axis=0)
-        pieces = [own, shift(own, dy=1), shift(own, dy=2), shift(own, dy=-1)]
-        late = assemble(numbers[3:4], pieces, batch, width, late)
-    mix_w, down_w = late
+        pieces += [own, shift(own, dy=1), shift(own, dy=2), shift(own, dy=-1)]
+    mix_w, down_w = assemble(numbers[3:4], pieces, width)
 
     stream = lax.dynamic_slice_in_dim(tokens, tp_at * own_rows, own_rows, 0)
     stream = rolled(stream, first_block).astype(F32)
-    parts = shares_of_rows(*down(gated([x], payloads, width), down_w))
-    stream, normed = settle(parts, stream, gain[1], gain[2], 0.5)
+    hidden = silu(total)
+    parts = shares_of_rows(*down(hidden, down_w))
+    stream, copies = settle(parts, stream, gains, 1, 0.5)
     kind = jnp.stack([numbers[2], numbers[1]])
-    share = mixer(kind, *rows_of_all(normed), mix_w, pool_w[0], pool_scale[None])
-    stream, normed = settle(shares_of_rows(*share), stream, gain[3], gain[4], 1.0)
-    hidden = gated(rows_of_all(normed), payloads, width)
+    share = mixer(kind, *rows_of_all(copies), mix_w, pool_w[0], pool_scale[None])
+    stream, copies = settle(shares_of_rows(*share), stream, gains, 3, 1.0)
+    hidden = gated(rows_of_all(copies), payloads, width)
     parts = shares_of_rows(*down(hidden, down_w))
-    return finish(numbers[0:1], parts, stream, gain[5])
+    return finish(numbers[0:1], parts, stream, gains)
 
 
 def solution(mesh):

time: 268 us -> 267 us (level)
  Pallas kernels: 18.4 us -> 23.4 us
  starting transfers between devices: 118 us -> 113 us
  blocking collectives: 59.3 us -> 62.3 us
    all_to_all x0 -> x2, blocking collectives: none -> 24.9 us  [rows_of_all(): lax.all_to_all(copies, 'tp', 0, 0, tiled=True, axis_index_groups=X_GROUPS)]
    all_gather x2 -> x0, blocking collectives: 22 us -> none  [rows_of_all(): lax.all_gather(normed, 'tp', axis=0, tiled=True, axis_index_groups=X_GROUPS)]
    pallas_call x4 -> x12, Pallas kernels: 3.38 us -> 9.97 us  [the longest x8 5.87 us: absorb(): pl.pallas_call(functools.partial(absorb_kernel, places), out_shape=jax.Sh...]
    ppermute x5, starting transfers between devices: 37.8 us -> 34 us  [core_swap(): return lax.ppermute(array, 'tp', [(k, k ^ 1) for k in range(8)])]
    ppermute x22, waiting for transfers between devices: 21.8 us -> 18.6 us  [shift(): return lax.ppermute(array, 'fs', fs_shift(dy, dz))]
    pallas_call x2 -> x1, Pallas kernels: 5.39 us -> 3.84 us  [gated(): pl.pallas_call(functools.partial(gated_kernel, width, len(xs)), out_shape...]
    unnamed x150 -> x110, local copies, waits for them, and re-layouts: 23.2 us -> 23.4 us
  transfers between devices with their start and end apart: 28 -> 28, of which waited for: 17 -> 13; matrix products, arithmetic and copies ran while one was open for 2% -> 5% of each run, Pallas kernels for 1% -> 3%
where the time goes in v2:
time: 267 us; the launch traced here: 266 us
  starting transfers between devices  113 us (42%)
  blocking collectives  62.3 us (23%)
  waiting for transfers between devices  36.8 us (14%)
  local copies, waits for them, and re-layouts  27.1 us (10%)
  Pallas kernels  23.4 us (9%)
    ppermute x22, starting transfers between devices, shift(): return lax.ppermute(array, 'fs', fs_shift(dy, dz))  75.2 us
    ppermute x5, starting transfers between devices, core_swap(): return lax.ppermute(array, 'tp', [(k, k ^ 1) for k in range(8)])  34 us
    all_to_all x2, blocking collectives, shares_of_rows(): lax.all_to_all(tiles, 'tp', 0, 0, tiled=True, axis_index_groups=X_GROUPS)  26.2 us
    all_to_all x2, blocking collectives, rows_of_all(): lax.all_to_all(copies, 'tp', 0, 0, tiled=True, axis_index_groups=X_GROUPS)  24.9 us
    unnamed x110, local copies, waits for them, and re-layouts  23.4 us
    ppermute x22, waiting for transfers between devices, shift(): return lax.ppermute(array, 'fs', fs_shift(dy, dz))  18.6 us
    all_gather x1, blocking collectives, body(): lax.all_gather(first, 'fs', axis=0, tiled=True, axis_index_groups=groups)  11.2 us
    all_to_all x1, waiting for transfers between devices, shares_of_rows(): lax.all_to_all(tiles, 'tp', 0, 0, tiled=True, axis_index_groups=X_GROUPS)  9.42 us
  transfers between devices with their start and end apart: 28, of which 13 were waited for; matrix products, arithmetic and copies ran while one was open for 5% of the time, Pallas kernels for 3%

profile of v2, /device:TPU:1, one launch (start us, length us, event | category | flops | bytes accessed | tf_op | source)
XLA Modules:
  0.0 265.7 jit_solution(14488757552183929213)
XLA Ops:
  1.7 11.2 %all_gather.3 = bf16[128,1408]{1,0:T(8,128)(2,1)S(1)} all-gather(bf16[32,1408]{1,0:T(8,128)(2,1)} %get-tuple-element.21), channel_id=1, replica_groups={{0,8,16,24},{32,40,48,56},{64,72,80,88},{96,104,112,120},{128,136,144,1..., dimensions={0}, use_global_device_ids=true | all-gather | bytes 450560 | tf_op jit(solution)/shard_map/all_gather | solution.py:400
  13.9 4.5 %collective-permute-start = (bf16[160,1408]{1,0:T(8,128)(2,1)S(1)}, bf16[160,1408]{1,0:T(8,128)(2,1)S(1)}, u32[]{:S(2)}, u32[]{:S(2)}) collective-permute-start(bf16[160,1408]{1,0:T(8,128)(2,1)S(1)} %constant_dynamic-update-slice_fusion.refs_0_.refs_10_), channel_id=1, source_target_pairs={{0,32},{8,40},{16,48},{24,56},{32,64},{40,72},{48,80},{56,88},{64,... | collective-permute-start | bytes 1351688 | tf_op jit(solution)/shard_map/ppermute | solution.py:35
  18.4 9.5 %collective-permute-start.8 = (bf16[160,1408]{1,0:T(8,128)(2,1)S(1)}, bf16[160,1408]{1,0:T(8,128)(2,1)S(1)}, u32[]{:S(2)}, u32[]{:S(2)}) collective-permute-start(bf16[160,1408]{1,0:T(8,128)(2,1)S(1)} %constant_dynamic-update-slice_fusion.refs_0_.refs_10_), channel_id=1, source_target_pairs={{0,480},{8,488},{16,496},{24,504},{32,0},{40,8},{48,16},{56,24},{6... | collective-permute-start | bytes 1351688 | tf_op jit(solution)/shard_map/ppermute | solution.py:35
  28.7 5.4 %collective-permute-done.refs_1_.refs_9_ = bf16[160,1408]{1,0:T(8,128)(2,1)S(1)} collective-permute-done((bf16[160,1408]{1,0:T(8,128)(2,1)S(1)}, bf16[160,1408]{1,0:T(8,128)(2,1)S(1)}, u32[]{:S(2)}, u32[]{:S(2)}) %collective-permute-start) | collective-permute-done | bytes 450592 | tf_op jit(solution)/shard_map/ppermute | solution.py:35
  36.1 4.6 %collective-permute-start.9 = (bf16[160,1408]{1,0:T(8,128)(2,1)S(1)}, bf16[160,1408]{1,0:T(8,128)(2,1)S(1)}, u32[]{:S(2)}, u32[]{:S(2)}) collective-permute-start(bf16[160,1408]{1,0:T(8,128)(2,1)S(1)} %collective-permute-done.8.refs_2_.refs_11_), channel_id=1, source_target_pairs={{0,480},{8,488},{16,496},{24,504},{32,0},{40,8},{48,16},{56,24},{6... | collective-permute-start | bytes 1351688 | tf_op jit(solution)/shard_map/ppermute | solution.py:35
  41.9 4.1 %collective-permute-done.1.refs_0_.refs_8_ = bf16[160,1408]{1,0:T(8,128)(2,1)S(1)} collective-permute-done((bf16[160,1408]{1,0:T(8,128)(2,1)S(1)}, bf16[160,1408]{1,0:T(8,128)(2,1)S(1)}, u32[]{:S(2)}, u32[]{:S(2)}) %collective-permute-start.1) | collective-permute-done | bytes 450592 | tf_op jit(solution)/shard_map/ppermute | solution.py:35
  47.9 4.6 %collective-permute-start.10 = (bf16[160,1408]{1,0:T(8,128)(2,1)S(1)}, bf16[160,1408]{1,0:T(8,128)(2,1)S(1)}, u32[]{:S(2)}, u32[]{:S(2)}) collective-permute-start(bf16[160,1408]{1,0:T(8,128)(2,1)S(1)} %collective-permute-done.9.refs_1_.refs_12_), channel_id=1, source_target_pairs={{0,480},{8,488},{16,496},{24,504},{32,0},{40,8},{48,16},{56,24},{6... | collective-permute-start | bytes 1351688 | tf_op jit(solution)/shard_map/ppermute | solution.py:35
  58.9 4.6 %collective-permute-start.11 = (bf16[160,1408]{1,0:T(8,128)(2,1)S(1)}, bf16[160,1408]{1,0:T(8,128)(2,1)S(1)}, u32[]{:S(2)}, u32[]{:S(2)}) collective-permute-start(bf16[160,1408]{1,0:T(8,128)(2,1)S(1)} %collective-permute-done.10.refs_1_.refs_13_), channel_id=1, source_target_pairs={{0,480},{8,488},{16,496},{24,504},{32,0},{40,8},{48,16},{56,24},{6... | collective-permute-start | bytes 1351688 | tf_op jit(solution)/shard_map/ppermute | solution.py:35
  69.2 4.6 %collective-permute-start.12 = (bf16[160,1408]{1,0:T(8,128)(2,1)S(1)}, bf16[160,1408]{1,0:T(8,128)(2,1)S(1)}, u32[]{:S(2)}, u32[]{:S(2)}) collective-permute-start(bf16[160,1408]{1,0:T(8,128)(2,1)S(1)} %collective-permute-done.11.refs_1_.refs_14_), channel_id=1, source_target_pairs={{0,480},{8,488},{16,496},{24,504},{32,0},{40,8},{48,16},{56,24},{6... | collective-permute-start | bytes 1351688 | tf_op jit(solution)/shard_map/ppermute | solution.py:35
  79.6 4.7 %collective-permute-start.13 = (bf16[160,1408]{1,0:T(8,128)(2,1)S(1)}, bf16[160,1408]{1,0:T(8,128)(2,1)S(1)}, u32[]{:S(2)}, u32[]{:S(2)}) collective-permute-start(bf16[160,1408]{1,0:T(8,128)(2,1)S(1)} %collective-permute-done.12.refs_1_.refs_15_), channel_id=1, source_target_pairs={{0,480},{8,488},{16,496},{24,504},{32,0},{40,8},{48,16},{56,24},{6... | collective-permute-start | bytes 1351688 | tf_op jit(solution)/shard_map/ppermute | solution.py:35
  89.1 3.6 %collective-permute-start.16 = (bf16[352,960]{1,0:T(8,128)(2,1)}, bf16[352,960]{1,0:T(8,128)(2,1)S(1)}, u32[]{:S(2)}, u32[]{:S(2)}) collective-permute-start(bf16[352,960]{1,0:T(8,128)(2,1)} %slice_dynamic-update-slice_fusion.3.refs_0_), channel_id=1, source_target_pairs={{0,16},{8,24},{16,0},{24,8},{32,48},{40,56},{48,32},{56,40},{64,80... | collective-permute-start | bytes 2027528 | tf_op jit(solution)/shard_map/ppermute | solution.py:35
  98.1 4.6 %collective-permute-start.14 = (bf16[160,1408]{1,0:T(8,128)(2,1)S(1)}, bf16[160,1408]{1,0:T(8,128)(2,1)S(1)}, u32[]{:S(2)}, u32[]{:S(2)}) collective-permute-start(bf16[160,1408]{1,0:T(8,128)(2,1)S(1)} %collective-permute-done.13.refs_1_.refs_16_), channel_id=1, source_target_pairs={{0,480},{8,488},{16,496},{24,504},{32,0},{40,8},{48,16},{56,24},{6... | collective-permute-start | bytes 1351688 | tf_op jit(solution)/shard_map/ppermute | solution.py:35
  118.0 3.5 %collective-permute-start.20 = (bf16[160,960]{1,0:T(8,128)(2,1)}, bf16[160,960]{1,0:T(8,128)(2,1)}, u32[]{:S(2)}, u32[]{:S(2)}) collective-permute-start(bf16[160,960]{1,0:T(8,128)(2,1)} %constant_dynamic-update-slice_fusion.2.refs_4_), channel_id=1, source_target_pairs={{0,16},{8,24},{16,0},{24,8},{32,48},{40,56},{48,32},{56,40},{64,80... | collective-permute-start | bytes 921608 | tf_op jit(solution)/shard_map/ppermute | solution.py:35
  122.4 4.0 %collective-permute-start.21 = (bf16[160,960]{1,0:T(8,128)(2,1)}, bf16[160,960]{1,0:T(8,128)(2,1)}, u32[]{:S(2)}, u32[]{:S(2)}) collective-permute-start(bf16[160,960]{1,0:T(8,128)(2,1)} %constant_dynamic-update-slice_fusion.2.refs_4_), channel_id=1, source_target_pairs={{0,24},{8,0},{16,8},{24,16},{32,56},{40,32},{48,40},{56,48},{64,88... | collective-permute-start | bytes 921608 | tf_op jit(solution)/shard_map/ppermute | solution.py:35
  142.5 21.0 %collective-permute-start.22 = (bf16[160,2048]{1,0:T(8,128)(2,1)S(1)}, bf16[160,2048]{1,0:T(8,128)(2,1)S(1)}, u32[]{:S(2)}, u32[]{:S(2)}) collective-permute-start(bf16[160,2048]{1,0:T(8,128)(2,1)S(1)} %get-tuple-element.27), channel_id=1, source_target_pairs={{0,1},{1,0},{2,3},{3,2},{4,5},{5,4},{6,7},{7,6},{8,9},{9,8},{10,11... | collective-permute-start | bytes 1966088 | tf_op jit(solution)/shard_map/ppermute | solution.py:375
  166.3 4.2 %all-to-all-start = ((bf16[4,40,2048]{2,1,0:T(8,128)(2,1)}), bf16[4,40,2048]{2,1,0:T(8,128)(2,1)}, u32[]{:S(2)}, u32[]{:S(2)}) async-start(bf16[4,40,2048]{2,1,0:T(8,128)(2,1)} %bitcast.17), calls=%async_computation | async-start | bytes 1310720 | tf_op jit(solution)/shard_map/all_to_all | solution.py:381
  171.6 9.4 %all-to-all-done.parts_ref = bf16[4,40,2048]{2,1,0:T(8,128)(2,1)} async-done(((bf16[4,40,2048]{2,1,0:T(8,128)(2,1)}), bf16[4,40,2048]{2,1,0:T(8,128)(2,1)}, u32[]{:S(2)}, u32[]{:S(2)}) %all-to-all-start) | async-done | bytes 655392 | tf_op jit(solution)/shard_map/all_to_all | solution.py:381
  182.4 12.4 %all_to_all.25 = bf16[4,40,2048]{2,1,0:T(8,128)(2,1)} all-to-all(bf16[4,40,2048]{2,1,0:T(8,128)(2,1)S(1)} %get-tuple-element.28), channel_id=1, replica_groups={{0,2,4,6},{1,3,5,7},{8,10,12,14},{9,11,13,15},{16,18,20,22},{17,19,21,2..., dimensions={0} | all-to-all | bytes 1310720 | tf_op jit(solution)/shard_map/all_to_all | solution.py:385
  194.8 4.4 %collective-permute-start.23 = (bf16[160,2048]{1,0:T(8,128)(2,1)}, bf16[160,2048]{1,0:T(8,128)(2,1)}, u32[]{:S(2)}, u32[]{:S(2)}) collective-permute-start(bf16[160,2048]{1,0:T(8,128)(2,1)} %bitcast.7.mine_ref), channel_id=1, source_target_pairs={{0,1},{1,0},{2,3},{3,2},{4,5},{5,4},{6,7},{7,6},{8,9},{9,8},{10,11... | collective-permute-start | bytes 1966088 | tf_op jit(solution)/shard_map/ppermute | solution.py:375
  210.7 13.1 %all_to_all.26.parts_ref = bf16[4,40,2048]{2,1,0:T(8,128)(2,1)S(1)} all-to-all(bf16[4,40,2048]{2,1,0:T(8,128)(2,1)S(1)} %bitcast.18), channel_id=1, replica_groups={{0,2,4,6},{1,3,5,7},{8,10,12,14},{9,11,13,15},{16,18,20,22},{17,19,21,2..., dimensions={0} | all-to-all | bytes 1310720 | tf_op jit(solution)/shard_map/all_to_all | solution.py:381
  224.2 12.5 %all_to_all.27 = bf16[4,40,2048]{2,1,0:T(8,128)(2,1)S(1)} all-to-all(bf16[4,40,2048]{2,1,0:T(8,128)(2,1)S(1)} %get-tuple-element.33), channel_id=1, replica_groups={{0,2,4,6},{1,3,5,7},{8,10,12,14},{9,11,13,15},{16,18,20,22},{17,19,21,2..., dimensions={0} | all-to-all | bytes 1310720 | tf_op jit(solution)/shard_map/all_to_all | solution.py:385
  236.7 4.0 %collective-permute-start.25 = (bf16[160,2048]{1,0:T(8,128)(2,1)S(1)}, bf16[160,2048]{1,0:T(8,128)(2,1)S(1)}, u32[]{:S(2)}, u32[]{:S(2)}) collective-permute-start(bf16[160,2048]{1,0:T(8,128)(2,1)S(1)} %bitcast.13), channel_id=1, source_target_pairs={{0,1},{1,0},{2,3},{3,2},{4,5},{5,4},{6,7},{7,6},{8,9},{9,8},{10,11... | collective-permute-start | bytes 1966088 | tf_op jit(solution)/shard_map/ppermute | solution.py:375
  242.5 3.8 %gated.1.h_ref = bf16[320,704]{1,0:T(8,128)(2,1)S(1)} custom-call(bf16[160,2048]{1,0:T(8,128)(2,1)S(1)} %bitcast.14, bf16[160,2048]{1,0:T(8,128)(2,1)S(1)} %collective-permute-done.25.refs_1_, bf16[160,1408]{1,0:T(8,128)(2,1)} %collective-permute-done.7.refs_0_.refs_2_, bf16[160,1408]{1,0:T(8,128)(2,1)} %collective-permute-done.6.refs_0_.refs_3_, ...), custom_call_target="tpu_custom_call" | custom-call | flops 1845493760 | bytes 8388608 | tf_op jit(solution)/shard_map/gated/pallas_call | solution.py:199
  251.8 13.0 %all_to_all.28.parts_ref = bf16[4,40,2048]{2,1,0:T(8,128)(2,1)S(1)} all-to-all(bf16[4,40,2048]{2,1,0:T(8,128)(2,1)S(1)} %bitcast.19), channel_id=1, replica_groups={{0,2,4,6},{1,3,5,7},{8,10,12,14},{9,11,13,15},{16,18,20,22},{17,19,21,2..., dimensions={0} | all-to-all | bytes 1310720 | tf_op jit(solution)/shard_map/all_to_all | solution.py:381
  (178 shorter events, 93.5 us)
Async XLA Ops:
  13.9 20.2 %collective-permute-start = (bf16[160,1408]{1,0:T(8,128)(2,1)S(1)}, bf16[160,1408]{1,0:T(8,128)(2,1)S(1)}, u32[]{:S(2)}, u32[]{:S(2)}) collective-permute-start(bf16[160,1408]{1,0:T(8,128)(2,1)S(1)} %constant_dynamic-update-slice_fusion.refs_0_.refs_10_), channel_id=1, source_target_pairs={{0,32},{8,40},{16,48},{24,56},{32,64},{40,72},{48,80},{56,88},{64,... | collective-permute-start | bytes 1351688 | tf_op jit(solution)/shard_map/ppermute | solution.py:35
  18.4 17.6 %collective-permute-start.8 = (bf16[160,1408]{1,0:T(8,128)(2,1)S(1)}, bf16[160,1408]{1,0:T(8,128)(2,1)S(1)}, u32[]{:S(2)}, u32[]{:S(2)}) collective-permute-start(bf16[160,1408]{1,0:T(8,128)(2,1)S(1)} %constant_dynamic-update-slice_fusion.refs_0_.refs_10_), channel_id=1, source_target_pairs={{0,480},{8,488},{16,496},{24,504},{32,0},{40,8},{48,16},{56,24},{6... | collective-permute-start | bytes 1351688 | tf_op jit(solution)/shard_map/ppermute | solution.py:35
  34.1 11.8 %collective-permute-start.1 = (bf16[160,1408]{1,0:T(8,128)(2,1)S(1)}, bf16[160,1408]{1,0:T(8,128)(2,1)S(1)}, u32[]{:S(2)}, u32[]{:S(2)}) collective-permute-start(bf16[160,1408]{1,0:T(8,128)(2,1)S(1)} %collective-permute-done.refs_1_.refs_9_), channel_id=1, source_target_pairs={{0,32},{8,40},{16,48},{24,56},{32,64},{40,72},{48,80},{56,88},{64,... | collective-permute-start | bytes 1351688 | tf_op jit(solution)/shard_map/ppermute | solution.py:35
  36.1 11.8 %collective-permute-start.9 = (bf16[160,1408]{1,0:T(8,128)(2,1)S(1)}, bf16[160,1408]{1,0:T(8,128)(2,1)S(1)}, u32[]{:S(2)}, u32[]{:S(2)}) collective-permute-start(bf16[160,1408]{1,0:T(8,128)(2,1)S(1)} %collective-permute-done.8.refs_2_.refs_11_), channel_id=1, source_target_pairs={{0,480},{8,488},{16,496},{24,504},{32,0},{40,8},{48,16},{56,24},{6... | collective-permute-start | bytes 1351688 | tf_op jit(solution)/shard_map/ppermute | solution.py:35
  46.0 11.0 %collective-permute-start.2 = (bf16[160,1408]{1,0:T(8,128)(2,1)S(1)}, bf16[160,1408]{1,0:T(8,128)(2,1)S(1)}, u32[]{:S(2)}, u32[]{:S(2)}) collective-permute-start(bf16[160,1408]{1,0:T(8,128)(2,1)S(1)} %collective-permute-done.1.refs_0_.refs_8_), channel_id=1, source_target_pairs={{0,32},{8,40},{16,48},{24,56},{32,64},{40,72},{48,80},{56,88},{64,... | collective-permute-start | bytes 1351688 | tf_op jit(solution)/shard_map/ppermute | solution.py:35
  47.9 11.0 %collective-permute-start.10 = (bf16[160,1408]{1,0:T(8,128)(2,1)S(1)}, bf16[160,1408]{1,0:T(8,128)(2,1)S(1)}, u32[]{:S(2)}, u32[]{:S(2)}) collective-permute-start(bf16[160,1408]{1,0:T(8,128)(2,1)S(1)} %collective-permute-done.9.refs_1_.refs_12_), channel_id=1, source_target_pairs={{0,480},{8,488},{16,496},{24,504},{32,0},{40,8},{48,16},{56,24},{6... | collective-permute-start | bytes 1351688 | tf_op jit(solution)/shard_map/ppermute | solution.py:35
  57.0 10.3 %collective-permute-start.3 = (bf16[160,1408]{1,0:T(8,128)(2,1)S(1)}, bf16[160,1408]{1,0:T(8,128)(2,1)S(1)}, u32[]{:S(2)}, u32[]{:S(2)}) collective-permute-start(bf16[160,1408]{1,0:T(8,128)(2,1)S(1)} %collective-permute-done.2.refs_0_.refs_7_), channel_id=1, source_target_pairs={{0,32},{8,40},{16,48},{24,56},{32,64},{40,72},{48,80},{56,88},{64,... | collective-permute-start | bytes 1351688 | tf_op jit(solution)/shard_map/ppermute | solution.py:35
  58.9 10.3 %collective-permute-start.11 = (bf16[160,1408]{1,0:T(8,128)(2,1)S(1)}, bf16[160,1408]{1,0:T(8,128)(2,1)S(1)}, u32[]{:S(2)}, u32[]{:S(2)}) collective-permute-start(bf16[160,1408]{1,0:T(8,128)(2,1)S(1)} %collective-permute-done.10.refs_1_.refs_13_), channel_id=1, source_target_pairs={{0,480},{8,488},{16,496},{24,504},{32,0},{40,8},{48,16},{56,24},{6... | collective-permute-start | bytes 1351688 | tf_op jit(solution)/shard_map/ppermute | solution.py:35
  67.3 10.3 %collective-permute-start.4 = (bf16[160,1408]{1,0:T(8,128)(2,1)S(1)}, bf16[160,1408]{1,0:T(8,128)(2,1)S(1)}, u32[]{:S(2)}, u32[]{:S(2)}) collective-permute-start(bf16[160,1408]{1,0:T(8,128)(2,1)S(1)} %collective-permute-done.3.refs_0_.refs_6_), channel_id=1, source_target_pairs={{0,32},{8,40},{16,48},{24,56},{32,64},{40,72},{48,80},{56,88},{64,... | collective-permute-start | bytes 1351688 | tf_op jit(solution)/shard_map/ppermute | solution.py:35
  69.2 10.3 %collective-permute-start.12 = (bf16[160,1408]{1,0:T(8,128)(2,1)S(1)}, bf16[160,1408]{1,0:T(8,128)(2,1)S(1)}, u32[]{:S(2)}, u32[]{:S(2)}) collective-permute-start(bf16[160,1408]{1,0:T(8,128)(2,1)S(1)} %collective-permute-done.11.refs_1_.refs_14_), channel_id=1, source_target_pairs={{0,480},{8,488},{16,496},{24,504},{32,0},{40,8},{48,16},{56,24},{6... | collective-permute-start | bytes 1351688 | tf_op jit(solution)/shard_map/ppermute | solution.py:35
  77.6 18.5 %collective-permute-start.5 = (bf16[160,1408]{1,0:T(8,128)(2,1)S(1)}, bf16[160,1408]{1,0:T(8,128)(2,1)S(1)}, u32[]{:S(2)}, u32[]{:S(2)}) collective-permute-start(bf16[160,1408]{1,0:T(8,128)(2,1)S(1)} %collective-permute-done.4.refs_0_.refs_5_), channel_id=1, source_target_pairs={{0,32},{8,40},{16,48},{24,56},{32,64},{40,72},{48,80},{56,88},{64,... | collective-permute-start | bytes 1351688 | tf_op jit(solution)/shard_map/ppermute | solution.py:35
  79.6 18.5 %collective-permute-start.13 = (bf16[160,1408]{1,0:T(8,128)(2,1)S(1)}, bf16[160,1408]{1,0:T(8,128)(2,1)S(1)}, u32[]{:S(2)}, u32[]{:S(2)}) collective-permute-start(bf16[160,1408]{1,0:T(8,128)(2,1)S(1)} %collective-permute-done.12.refs_1_.refs_15_), channel_id=1, source_target_pairs={{0,480},{8,488},{16,496},{24,504},{32,0},{40,8},{48,16},{56,24},{6... | collective-permute-start | bytes 1351688 | tf_op jit(solution)/shard_map/ppermute | solution.py:35
  87.2 30.0 %collective-permute-start.15 = (bf16[352,960]{1,0:T(8,128)(2,1)}, bf16[352,960]{1,0:T(8,128)(2,1)S(1)}, u32[]{:S(2)}, u32[]{:S(2)}) collective-permute-start(bf16[352,960]{1,0:T(8,128)(2,1)} %slice_dynamic-update-slice_fusion.3.refs_0_), channel_id=1, source_target_pairs={{0,8},{8,16},{16,24},{24,0},{32,40},{40,48},{48,56},{56,32},{64,72... | collective-permute-start | bytes 2027528 | tf_op jit(solution)/shard_map/ppermute | solution.py:35
  89.1 32.5 %collective-permute-start.16 = (bf16[352,960]{1,0:T(8,128)(2,1)}, bf16[352,960]{1,0:T(8,128)(2,1)S(1)}, u32[]{:S(2)}, u32[]{:S(2)}) collective-permute-start(bf16[352,960]{1,0:T(8,128)(2,1)} %slice_dynamic-update-slice_fusion.3.refs_0_), channel_id=1, source_target_pairs={{0,16},{8,24},{16,0},{24,8},{32,48},{40,56},{48,32},{56,40},{64,80... | collective-permute-start | bytes 2027528 | tf_op jit(solution)/shard_map/ppermute | solution.py:35
  92.7 43.8 %collective-permute-start.17 = (bf16[352,960]{1,0:T(8,128)(2,1)}, bf16[352,960]{1,0:T(8,128)(2,1)}, u32[]{:S(2)}, u32[]{:S(2)}) collective-permute-start(bf16[352,960]{1,0:T(8,128)(2,1)} %slice_dynamic-update-slice_fusion.3.refs_0_), channel_id=1, source_target_pairs={{0,24},{8,0},{16,8},{24,16},{32,56},{40,32},{48,40},{56,48},{64,88... | collective-permute-start | bytes 2027528 | tf_op jit(solution)/shard_map/ppermute | solution.py:35
  96.2 10.6 %collective-permute-start.6 = (bf16[160,1408]{1,0:T(8,128)(2,1)S(1)}, bf16[160,1408]{1,0:T(8,128)(2,1)}, u32[]{:S(2)}, u32[]{:S(2)}) collective-permute-start(bf16[160,1408]{1,0:T(8,128)(2,1)S(1)} %collective-permute-done.5.refs_0_.refs_4_), channel_id=1, source_target_pairs={{0,32},{8,40},{16,48},{24,56},{32,64},{40,72},{48,80},{56,88},{64,... | collective-permute-start | bytes 1351688 | tf_op jit(solution)/shard_map/ppermute | solution.py:35
  98.1 12.1 %collective-permute-start.14 = (bf16[160,1408]{1,0:T(8,128)(2,1)S(1)}, bf16[160,1408]{1,0:T(8,128)(2,1)S(1)}, u32[]{:S(2)}, u32[]{:S(2)}) collective-permute-start(bf16[160,1408]{1,0:T(8,128)(2,1)S(1)} %collective-permute-done.13.refs_1_.refs_16_), channel_id=1, source_target_pairs={{0,480},{8,488},{16,496},{24,504},{32,0},{40,8},{48,16},{56,24},{6... | collective-permute-start | bytes 1351688 | tf_op jit(solution)/shard_map/ppermute | solution.py:35
  106.8 7.8 %collective-permute-start.18 = (bf16[32,960]{1,0:T(8,128)(2,1)S(1)}, bf16[32,960]{1,0:T(8,128)(2,1)S(1)}, u32[]{:S(2)}, u32[]{:S(2)}) collective-permute-start(bf16[32,960]{1,0:T(8,128)(2,1)S(1)} %get-tuple-element.37), channel_id=1, source_target_pairs={{0,64},{8,72},{16,80},{24,88},{32,96},{40,104},{48,112},{56,120},{... | collective-permute-start | bytes 184328 | tf_op jit(solution)/shard_map/ppermute | solution.py:35
  110.2 29.3 %collective-permute-start.7 = (bf16[160,1408]{1,0:T(8,128)(2,1)}, bf16[160,1408]{1,0:T(8,128)(2,1)}, u32[]{:S(2)}, u32[]{:S(2)}) collective-permute-start(bf16[160,1408]{1,0:T(8,128)(2,1)} %collective-permute-done.6.refs_0_.refs_3_), channel_id=1, source_target_pairs={{0,32},{8,40},{16,48},{24,56},{32,64},{40,72},{48,80},{56,88},{64,... | collective-permute-start | bytes 1351688 | tf_op jit(solution)/shard_map/ppermute | solution.py:35
  115.2 21.2 %collective-permute-start.19 = (bf16[160,960]{1,0:T(8,128)(2,1)}, bf16[160,960]{1,0:T(8,128)(2,1)}, u32[]{:S(2)}, u32[]{:S(2)}) collective-permute-start(bf16[160,960]{1,0:T(8,128)(2,1)} %constant_dynamic-update-slice_fusion.2.refs_4_), channel_id=1, source_target_pairs={{0,8},{8,16},{16,24},{24,0},{32,40},{40,48},{48,56},{56,32},{64,72... | collective-permute-start | bytes 921608 | tf_op jit(solution)/shard_map/ppermute | solution.py:35
  118.0 18.4 %collective-permute-start.20 = (bf16[160,960]{1,0:T(8,128)(2,1)}, bf16[160,960]{1,0:T(8,128)(2,1)}, u32[]{:S(2)}, u32[]{:S(2)}) collective-permute-start(bf16[160,960]{1,0:T(8,128)(2,1)} %constant_dynamic-update-slice_fusion.2.refs_4_), channel_id=1, source_target_pairs={{0,16},{8,24},{16,0},{24,8},{32,48},{40,56},{48,32},{56,40},{64,80... | collective-permute-start | bytes 921608 | tf_op jit(solution)/shard_map/ppermute | solution.py:35
  122.4 14.1 %collective-permute-start.21 = (bf16[160,960]{1,0:T(8,128)(2,1)}, bf16[160,960]{1,0:T(8,128)(2,1)}, u32[]{:S(2)}, u32[]{:S(2)}) collective-permute-start(bf16[160,960]{1,0:T(8,128)(2,1)} %constant_dynamic-update-slice_fusion.2.refs_4_), channel_id=1, source_target_pairs={{0,24},{8,0},{16,8},{24,16},{32,56},{40,32},{48,40},{56,48},{64,88... | collective-permute-start | bytes 921608 | tf_op jit(solution)/shard_map/ppermute | solution.py:35
  142.5 22.7 %collective-permute-start.22 = (bf16[160,2048]{1,0:T(8,128)(2,1)S(1)}, bf16[160,2048]{1,0:T(8,128)(2,1)S(1)}, u32[]{:S(2)}, u32[]{:S(2)}) collective-permute-start(bf16[160,2048]{1,0:T(8,128)(2,1)S(1)} %get-tuple-element.27), channel_id=1, source_target_pairs={{0,1},{1,0},{2,3},{3,2},{4,5},{5,4},{6,7},{7,6},{8,9},{9,8},{10,11... | collective-permute-start | bytes 1966088 | tf_op jit(solution)/shard_map/ppermute | solution.py:375
  166.3 14.7 %all-to-all-start = ((bf16[4,40,2048]{2,1,0:T(8,128)(2,1)}), bf16[4,40,2048]{2,1,0:T(8,128)(2,1)}, u32[]{:S(2)}, u32[]{:S(2)}) async-start(bf16[4,40,2048]{2,1,0:T(8,128)(2,1)} %bitcast.17), calls=%async_computation | async-start | bytes 1310720 | tf_op jit(solution)/shard_map/all_to_all | solution.py:381
  (52 other events, 1167.9 us)
